TPU v7x, 512 devices: a whole 4x4x16 slice. The times are simulated.
512 devices in a mesh: sp: 128 (over z, x, core), tp: 4 (over y).
Axes of the slice: x: 4, y: 4, z: 16, core: 2. Of those that a mesh axis runs over, the one named last changes fastest.
Arguments:
- inputs: bfloat16 [32768, 2048], P('sp', 'tp'), may hold values from -120 to 120
- in_gain: float32 [2048], replicated, may hold values from 0.1 to 1.9
- query_weight: bfloat16 [2048, 1024], P('sp', 'tp'), may hold values from -0.125 to 0.125
- key_weight: bfloat16 [2048, 1024], P('sp', 'tp'), may hold values from -0.125 to 0.125
- value_weight: bfloat16 [2048, 1024], P('sp', 'tp'), may hold values from -0.125 to 0.125
- beta_weight: bfloat16 [2, 2048, 8], replicated, may hold values from -0.125 to 0.125
- decay_weight: bfloat16 [2, 2048, 8], replicated, may hold values from -0.125 to 0.125
- beta_shift: float32 [2, 8], replicated, may hold values from -9 to 1
- decay_pace: float32 [2, 8, 32768], P(None, 'tp', 'sp'), may hold values from 0 to 0.1
- decay_jolt: float32 [2, 8, 32768], P(None, 'tp', 'sp'), may hold values from -1.4 to 0, as said below
- head_gain: float32 [128], replicated, may hold values from 0.1 to 1.9
- glu_value_weight: bfloat16 [2048, 1024], P('sp', 'tp'), may hold values from -0.125 to 0.125
- glu_gate_weight: bfloat16 [2048, 1024], P('sp', 'tp'), may hold values from -0.125 to 0.125
- conv_kernel: bfloat16 [31, 1024], P(None, 'tp'), may hold values from -4 to 4
- conv_gain: float32 [1024], P('tp'), may hold values from 0.1 to 1.9
- out_delta_weight: bfloat16 [1024, 2048], P('tp', 'sp'), may hold values from -0.125 to 0.125
- out_conv_weight: bfloat16 [1024, 2048], P('tp', 'sp'), may hold values from -0.125 to 0.125
Outputs:
- mixed: bfloat16 [32768, 2048], P(('sp', 'tp'))
Inputs may be any that keep to these rules, and one draw needn't show every extreme that they name: `decay_jolt`: zero but at a few positions of each direction and head.
All inputs are finite; a program needn't handle non-finite values.
Results may differ from a plain program's by a relative error of at most 0.017.
Values may be sent and summed in bfloat16 or wider, within the bound.
A program may use at most 128 MiB of HBM per device.

v0:
```python
import jax
import jax.numpy as jnp
from jax import lax
from jax.sharding import Mesh
from jax.sharding import PartitionSpec as P

HEAD = 128
QK_HEADS = 8
V_HEADS = 8
CONV_CH = 1024
KERNEL = 31
BLOCK = 64
SP = ("sp_0", "sp_1", "sp_2")
SP_TP = ("sp_0", "sp_1", "sp_2", "tp")


highest = lax.Precision.HIGHEST


def sent_to_all(shard, axis):
    copies = jnp.broadcast_to(shard, (lax.axis_size(axis), *shard.shape))
    return lax.all_to_all(copies, axis, split_axis=0, concat_axis=0, tiled=True)


def joined_along(tiles, dim):
    tiles = jnp.moveaxis(tiles, 0, dim)
    shape = tiles.shape
    return tiles.reshape(*shape[:dim], shape[dim] * shape[dim + 1], *shape[dim + 2 :])


def gather_directly(shard, axis, dim):
    tiles = sent_to_all(shard, axis)
    return joined_along(tiles, dim)


def side_by_side(arrays, axis, dim, along):
    ends, at = ([], 0)
    for a in arrays[:-1]:
        at += a.shape[along]
        ends.append(at)
    both = jnp.concatenate(arrays, axis=along)
    return tuple(jnp.split(lax.all_gather(both, axis, axis=dim, tiled=True), ends, axis=along))


def neutral_like(shard, identity):
    return jax.tree.map(
        lambda part, zero: jnp.zeros_like(part) + jnp.asarray(zero, part.dtype), shard, identity
    )


def prefix_by_axis(shard, axes, combine, identity, reverse):
    before = start = neutral_like(shard, identity)
    total = shard
    for axis in reversed(axes):
        peers, position = (lax.axis_size(axis), lax.axis_index(axis))
        pieces = jax.tree.map(
            lambda part, kind: lax.all_gather(part.astype(kind), axis),
            total,
            (jnp.bfloat16, jnp.bfloat16),
        )
        inside, total = (start, start)
        for k in reversed(range(peers)) if reverse else range(peers):
            passed = k > position if reverse else k < position
            total = combine(
                total, jax.tree.map(lambda part, own: part[k].astype(own.dtype), pieces, shard)
            )
            inside = jax.tree.map(lambda new, old: jnp.where(passed, new, old), total, inside)
        before = combine(inside, before)
    return before


def padded_2(cells, sides, width):
    for axis, dim in sides:
        count = lax.axis_size(axis)
        ends = count - 1
        head = lax.slice_in_dim(cells, 0, width, axis=dim)
        tail = lax.slice_in_dim(cells, cells.shape[dim] - width, cells.shape[dim], axis=dim)
        cells = jnp.concatenate(
            [
                lax.ppermute(tail, axis, [(i, (i + 1) % count) for i in range(ends)]),
                cells,
                lax.ppermute(head, axis, [((i + 1) % count, i) for i in range(ends)]),
            ],
            axis=dim,
        )
    return cells


def of_everyone(shard, axis):
    return sent_to_all(shard, axis).sum(axis=0)


def packed_total(arrays, axis):
    line, at, gathered = (jnp.concatenate([a.reshape(-1) for a in arrays]), 0, [])
    total = of_everyone(line, axis)
    for a in arrays:
        gathered.append(total[at : at + a.size].reshape(a.shape))
        at += a.size
    return tuple(gathered)


def gather_turned(arrays, axis, dims):
    turned = [jnp.moveaxis(a, dim, 0) for a, dim in zip(arrays, dims)]
    both = jnp.concatenate([t.reshape(len(t), -1) for t in turned], axis=1)
    out, at, gathered = (lax.all_gather(both, axis, axis=0, tiled=True), 0, [])
    for t, dim in zip(turned, dims):
        section = out[:, at : at + t[0].size].reshape(-1, *t.shape[1:])
        gathered.append(jnp.moveaxis(section, 0, dim))
        at += t[0].size
    return tuple(gathered)


def in_blocks(shard, dim, peers):
    shape = shard.shape
    tiles = shard.reshape(*shape[:dim], peers, shape[dim] // peers, *shape[dim + 1 :])
    return jnp.moveaxis(tiles, dim, 0)


def sent_and_summed(shard, axis, dim):
    tiles = in_blocks(shard, dim, lax.axis_size(axis))
    arrived = lax.all_to_all(tiles, axis, split_axis=0, concat_axis=0, tiled=True)
    return arrived.astype(jnp.float32).sum(axis=0)


def matmul_high(left_side, right_side):
    return jnp.matmul(left_side, right_side, precision=highest)


def unit_lower_inverse(matrix):
    order_size = matrix.shape[-1]
    leading = matrix.shape[:-2]
    inverse = jnp.ones(leading + (order_size, 1, 1), jnp.float32)
    size_now = 1
    while size_now < order_size:
        pair_count = order_size // (2 * size_now)
        halves = inverse.reshape(leading + (pair_count, 2, size_now, size_now))
        upper_inv = halves[..., 0, :, :]
        lower_inv = halves[..., 1, :, :]
        block_grid = matrix.reshape(leading + (pair_count, 2 * size_now, pair_count, 2 * size_now))
        diagonal = jnp.moveaxis(jnp.diagonal(block_grid, axis1=-4, axis2=-2), -1, -3)
        corner = diagonal[..., size_now:, :size_now]
        below = -matmul_high(lower_inv, matmul_high(corner, upper_inv))
        top_half = jnp.concatenate([upper_inv, jnp.zeros_like(below)], axis=-1)
        bottom_half = jnp.concatenate([below, lower_inv], axis=-1)
        inverse = jnp.concatenate([top_half, bottom_half], axis=-2)
        size_now = 2 * size_now
    return inverse.reshape(leading + (order_size, order_size))


def block_terms(queries, key_rows, values, beta_gate, log_decay):
    span = key_rows.shape[-2]
    cumulative = jnp.cumsum(log_decay, axis=-1)
    lower_mask = jnp.tril(jnp.ones((span, span), dtype=bool))
    strict = jnp.tril(jnp.ones((span, span), dtype=bool), -1)
    log_gap = cumulative[..., :, None] - cumulative[..., None, :]
    decay_mask = jnp.where(lower_mask, jnp.exp(jnp.where(lower_mask, log_gap, 0.0)), 0.0)
    key_inner = matmul_high(key_rows, jnp.swapaxes(key_rows, -1, -2))
    below_part = jnp.where(strict, beta_gate[..., :, None] * key_inner * decay_mask, 0.0)
    inverse = unit_lower_inverse(below_part + jnp.eye(span, dtype=jnp.float32))
    fresh = matmul_high(inverse, values * beta_gate[..., None])
    weighted = matmul_high(inverse, key_rows * (beta_gate * jnp.exp(cumulative))[..., None])
    scores = matmul_high(queries, jnp.swapaxes(key_rows, -1, -2)) * decay_mask
    readout = queries * jnp.exp(cumulative)[..., None] - matmul_high(scores, weighted)
    tail_keys = jnp.swapaxes(
        key_rows * jnp.exp(cumulative[..., -1:] - cumulative)[..., None], -1, -2
    )
    identity = jnp.eye(key_rows.shape[-1], dtype=jnp.float32)
    carry_map = jnp.exp(cumulative[..., -1])[..., None, None] * identity - matmul_high(
        tail_keys, weighted
    )
    carry_add = matmul_high(tail_keys, fresh)
    within = matmul_high(scores, fresh)
    return (carry_map, carry_add, readout, within)


def layer_norm_rows(inputs, gain):
    as_float = inputs.astype(jnp.float32)
    mean_row = jnp.mean(as_float, axis=-1, keepdims=True)
    spread = jnp.mean(jnp.square(as_float - mean_row), axis=-1, keepdims=True)
    return ((as_float - mean_row) * lax.rsqrt(spread + 1e-05) * gain).astype(jnp.bfloat16)


def compose(earlier, later):
    return (matmul_high(later[0], earlier[0]), matmul_high(later[0], earlier[1]) + later[1])


def local_maps(queries, key_rows, values, beta_gate, log_decay):
    head_count, length_dev, key_width = queries.shape
    value_width = values.shape[-1]
    block_count = length_dev // BLOCK

    def split_blocks(tensor):
        return tensor.reshape((head_count, block_count, BLOCK) + tensor.shape[2:])

    carry_map, carry_add, readout, within = block_terms(
        split_blocks(queries),
        split_blocks(key_rows),
        split_blocks(values),
        split_blocks(beta_gate),
        split_blocks(log_decay),
    )
    identity = jnp.broadcast_to(
        jnp.eye(key_width, dtype=jnp.float32), (head_count, key_width, key_width)
    )
    nothing = jnp.zeros((head_count, key_width, value_width), jnp.float32)

    def advance(prefix, block_parts):
        prefix_map, prefix_add = prefix
        step_map, step_add, step_read = block_parts
        reach_now = matmul_high(step_read, prefix_map)
        offset_now = matmul_high(step_read, prefix_add)
        return (
            (matmul_high(step_map, prefix_map), matmul_high(step_map, prefix_add) + step_add),
            (reach_now, offset_now),
        )

    moved = (
        jnp.moveaxis(carry_map, 1, 0),
        jnp.moveaxis(carry_add, 1, 0),
        jnp.moveaxis(readout, 1, 0),
    )
    totals, (reach_map, offset) = lax.scan(advance, (identity, nothing), moved)
    reach_map = jnp.moveaxis(reach_map, 0, 1).reshape(head_count, length_dev, key_width)
    offset = (jnp.moveaxis(offset, 0, 1) + within).reshape(head_count, length_dev, value_width)
    return (totals, reach_map, offset)


def on_device(
    inputs,
    in_gain,
    query_weight,
    key_weight,
    value_weight,
    beta_weight,
    decay_weight,
    beta_shift,
    decay_pace,
    decay_jolt,
    head_gain,
    glu_value_weight,
    glu_gate_weight,
    conv_kernel,
    conv_gain,
    out_delta_weight,
    out_conv_weight,
):
    gathered = gather_directly(inputs, "tp", 1)
    normed = layer_norm_rows(gathered, in_gain)
    row_count = normed.shape[0]

    def add_rows(shard_rows):
        return jnp.dot(normed, shard_rows, preferred_element_type=jnp.float32)

    def add_group(shards):
        return tuple((add_rows(shard_rows) for shard_rows in shards))

    delta_sums = add_group(side_by_side((query_weight, key_weight, value_weight), SP, 0, 1))
    conv_sums = add_group(side_by_side((glu_value_weight, glu_gate_weight), SP, 0, 1))
    queries, key_proj, value_proj = (summed.astype(jnp.bfloat16) for summed in delta_sums)
    local_heads = value_proj.shape[1] // HEAD
    group_size = V_HEADS // QK_HEADS
    head_first = lax.axis_index("tp") * local_heads

    def by_head(matrix, head_total):
        return jnp.transpose(
            matrix.astype(jnp.float32).reshape(row_count, head_total, HEAD), (1, 0, 2)
        )

    query_heads = jnp.repeat(
        jax.nn.silu(by_head(queries, local_heads // group_size)), group_size, axis=0
    )
    key_heads = jax.nn.silu(by_head(key_proj, local_heads // group_size))
    key_heads = key_heads * lax.rsqrt(
        jnp.sum(jnp.square(key_heads), axis=-1, keepdims=True) + 1e-06
    )
    key_heads = jnp.repeat(key_heads, group_size, axis=0)
    value_heads = by_head(value_proj, local_heads)
    own_beta = lax.dynamic_slice_in_dim(beta_weight, head_first, local_heads, 2)
    own_decay = lax.dynamic_slice_in_dim(decay_weight, head_first, local_heads, 2)
    beta_pre = jnp.einsum("td,edh->eht", normed, own_beta, preferred_element_type=jnp.float32)
    decay_pre = jnp.einsum("td,edh->eht", normed, own_decay, preferred_element_type=jnp.float32)
    own_shift = lax.dynamic_slice_in_dim(beta_shift, head_first, local_heads, 1)
    beta_gate = jax.nn.sigmoid(beta_pre + own_shift[:, :, None])
    log_decay = -decay_pace * jax.nn.softplus(decay_pre) + decay_jolt
    identity = jnp.broadcast_to(jnp.eye(HEAD, dtype=jnp.float32), (local_heads, HEAD, HEAD))
    nothing = jnp.zeros((local_heads, HEAD, HEAD), jnp.float32)
    forward_maps, forward_reach, forward_offset = local_maps(
        query_heads, key_heads, value_heads, beta_gate[0], log_decay[0]
    )
    entry_forward = prefix_by_axis(
        (forward_maps[0], forward_maps[1]), SP, compose, (identity, nothing), False
    )
    forward_out = matmul_high(forward_reach, entry_forward[1]) + forward_offset
    backward_maps, backward_reach, backward_offset = local_maps(
        jnp.flip(query_heads, 1),
        jnp.flip(key_heads, 1),
        jnp.flip(value_heads, 1),
        jnp.flip(beta_gate[1], 1),
        jnp.flip(log_decay[1], 1),
    )
    entry_backward = prefix_by_axis(
        (backward_maps[0], backward_maps[1]), SP, compose, (identity, nothing), True
    )
    backward_out = jnp.flip(matmul_high(backward_reach, entry_backward[1]) + backward_offset, 1)
    combined = forward_out + backward_out
    scaled = (
        combined
        * lax.rsqrt(jnp.mean(jnp.square(combined), axis=-1, keepdims=True) + 1e-06)
        * head_gain
    )
    delta_out = (
        jnp.transpose(scaled, (1, 0, 2)).reshape(row_count, local_heads * HEAD).astype(jnp.bfloat16)
    )
    glu_value, glu_gate = (summed.astype(jnp.bfloat16) for summed in conv_sums)
    gated = (glu_value.astype(jnp.float32) * jax.nn.sigmoid(glu_gate.astype(jnp.float32))).astype(
        jnp.bfloat16
    )
    padded = padded_2(gated, ((SP, 0),), KERNEL // 2)
    filtered = jnp.zeros(gated.shape, jnp.float32)
    for tap_index in range(KERNEL):
        filtered = filtered + padded[tap_index : tap_index + row_count].astype(
            jnp.float32
        ) * conv_kernel[tap_index].astype(jnp.float32)
    totals = packed_total((jnp.sum(filtered, axis=1), jnp.sum(filtered * filtered, axis=1)), "tp")
    mean_row = totals[0][:, None] / CONV_CH
    second = totals[1][:, None] / CONV_CH
    conv_out = jax.nn.silu(
        (filtered - mean_row) * lax.rsqrt(second - mean_row * mean_row + 1e-05) * conv_gain
    ).astype(jnp.bfloat16)
    delta_whole, conv_whole = gather_turned((out_delta_weight, out_conv_weight), SP, (1, 1))
    delta_part = jnp.dot(delta_out, delta_whole, preferred_element_type=jnp.float32)
    conv_part = jnp.dot(conv_out, conv_whole, preferred_element_type=jnp.float32)
    return sent_and_summed((delta_part + conv_part).astype(jnp.bfloat16), "tp", 0).astype(
        jnp.bfloat16
    )


def solution(mesh):
    finer = Mesh(mesh.devices.reshape(16, 4, 2, mesh.shape["tp"]), ("sp_0", "sp_1", "sp_2", "tp"))
    in_specs = (
        P(SP, "tp"),
        P(),
        P(SP, "tp"),
        P(SP, "tp"),
        P(SP, "tp"),
        P(),
        P(),
        P(),
        P(None, "tp", SP),
        P(None, "tp", SP),
        P(),
        P(SP, "tp"),
        P(SP, "tp"),
        P(None, "tp"),
        P("tp"),
        P("tp", SP),
        P("tp", SP),
    )
    out_specs = P(SP_TP, None)
    return jax.shard_map(
        on_device, mesh=finer, in_specs=in_specs, out_specs=out_specs, check_vma=False
    )
```

profile of v0, /device:TPU:1, one launch (start us, length us, event | category | flops | bytes accessed | tf_op | source)
XLA Modules:
  0.0 750.1 jit_solution(12263650205881839934)
XLA Ops:
  8.0 2.0 broadcast_in_dim.174
  10.0 5.0 all-to-all-start
  17.7 7.1 all-to-all-done
  32.3 125.3 %all-gather.20.cloned.1.call-done = bf16[2048,768]{1,0:T(8,128)(2,1)} async-done(((bf16[16,768]{1,0:T(8,128)(2,1)}), bf16[2048,768]{1,0:T(8,128)(2,1)}) %all-gather.20.cloned.1.call-update) | async-done | bytes 3145744 | tf_op jit(solution)/shard_map/all_gather | solution.py:42
  160.8 2.8 copy.415
  163.7 3.7 reshape.358
  167.4 2.0 reshape.360
  172.5 2.8 copy.384
  175.3 3.6 reshape.340
  186.0 4.8 copy.535
  190.8 2.9 gather_fusion
  193.8 4.8 copy.533
  198.6 2.9 gather_fusion.5
  203.6 6.3 copy.532
  209.8 2.9 gather_fusion.6
  215.4 1.8 copy.536
  217.2 2.2 gather_fusion.7
  221.4 2.4 copy.538
  232.1 2.1 convolution_bitcast_fusion.4
  235.8 8.0 %while.35 = (s32[]{:T(128)}, f32[2,128,128]{2,1,0:T(8,128)S(1)}, f32[2,128,128]{2,1,0:T(8,128)S(1)}, f32[4,2,64,128]{3,2,0,1:T(8,128)S(1)}, f32[4,2,64,128]{3,2,...) while((s32[]{:T(128)}, f32[2,128,128]{2,1,0:T(8,128)S(1)}, ...), condition=%wide.region_8.9_spmd.clone, body=%wide.region_7.8_spmd.clone.sunk | while | flops 151093248 | bytes 1970298 | solution.py:222
  244.6 1.9 all-gather.6
  248.7 6.2 copy.534
  254.9 3.0 gather_fusion.1
  262.6 1.9 reshape.342
  269.0 3.4 copy.537
  272.5 2.2 gather_fusion.2
  275.4 2.3 copy.539
  277.7 1.8 gather_fusion.3
  282.2 1.9 all-gather.9
  284.1 9.9 %all-gather.7 = bf16[8,128,128]{2,1,0:T(8,128)(2,1)S(1)} all-gather(bf16[2,128,128]{2,1,0:T(8,128)(2,1)S(1)} %get-tuple-element.371), channel_id=9, replica_groups=mesh['sp_0'=16,'sp_1'=4,'sp_2'=2,'tp'=4] {'sp_1'}, dimensions={0}, use_global_device_ids=true | all-gather | bytes 327680 | tf_op jit(solution)/shard_map/all_gather | solution.py:57
  302.0 9.4 %all-gather.10 = bf16[8,128,128]{2,1,0:T(8,128)(2,1)S(1)} all-gather(bf16[2,128,128]{2,1,0:T(8,128)(2,1)S(1)} %get-tuple-element.375), channel_id=12, replica_groups=mesh['sp_0'=16,'sp_1'=4,'sp_2'=2,'tp'=4] {'sp_1'}, dimensions={0}, use_global_device_ids=true | all-gather | bytes 327680 | tf_op jit(solution)/shard_map/all_gather | solution.py:57
  318.8 4.4 while.34
  323.2 7.2 all-gather
  331.5 9.8 %all-gather.1 = bf16[8,128,128]{2,1,0:T(8,128)(2,1)S(1)} all-gather(bf16[2,128,128]{2,1,0:T(8,128)(2,1)S(1)} %get-tuple-element.379), channel_id=3, replica_groups=mesh['sp_0'=16,'sp_1'=4,'sp_2'=2,'tp'=4] {'sp_1'}, dimensions={0}, use_global_device_ids=true | all-gather | bytes 327680 | tf_op jit(solution)/shard_map/all_gather | solution.py:57
  343.0 4.4 all-gather.3
  348.4 9.8 %all-gather.4 = bf16[8,128,128]{2,1,0:T(8,128)(2,1)S(1)} all-gather(bf16[2,128,128]{2,1,0:T(8,128)(2,1)S(1)} %get-tuple-element.383), channel_id=6, replica_groups=mesh['sp_0'=16,'sp_1'=4,'sp_2'=2,'tp'=4] {'sp_1'}, dimensions={0}, use_global_device_ids=true | all-gather | bytes 327680 | tf_op jit(solution)/shard_map/all_gather | solution.py:57
  360.4 1.8 fusion.68
  363.0 4.9 collective-permute-start.1
  367.9 2.2 collective-permute-start
  372.9 4.0 all-to-all-start.1
  377.7 3.3 all-to-all-done.1
  381.2 2.1 convolution_add_fusion.3
  389.0 41.1 %all-gather.32.cloned.1.call-done = bf16[32,128,128]{2,1,0:T(8,128)(2,1)} async-done(((bf16[2,128,128]{2,1,0:T(8,128)(2,1)}), bf16[32,128,128]{2,1,0:T(8,128)(2,1)}) %all-gather.32.cloned.1.call-update) | async-done | bytes 1048592 | tf_op jit(solution)/shard_map/all_gather | solution.py:57
  439.1 60.6 %all-gather.26.cloned.1.call-done = bf16[32,128,128]{2,1,0:T(8,128)(2,1)} async-done(((bf16[2,128,128]{2,1,0:T(8,128)(2,1)}), bf16[32,128,128]{2,1,0:T(8,128)(2,1)}) %all-gather.26.cloned.1.call-update) | async-done | bytes 1048592 | tf_op jit(solution)/shard_map/all_gather | solution.py:57
  499.7 69.6 %all-gather.28.cloned.1.call-done = bf16[32,128,128]{2,1,0:T(8,128)(2,1)} async-done(((bf16[2,128,128]{2,1,0:T(8,128)(2,1)}), bf16[32,128,128]{2,1,0:T(8,128)(2,1)}) %all-gather.28.cloned.1.call-update) | async-done | bytes 1048592 | tf_op jit(solution)/shard_map/all_gather | solution.py:57
  588.1 132.9 %all-gather.22.cloned.1.call-done = bf16[2048,512]{1,0:T(8,128)(2,1)} async-done(((bf16[16,512]{1,0:T(8,128)(2,1)}), bf16[2048,512]{1,0:T(8,128)(2,1)}) %all-gather.22.cloned.1.call-update) | async-done | bytes 2097168 | tf_op jit(solution)/shard_map/all_gather | solution.py:105
  721.0 1.9 fusion.82
  723.5 18.4 %all_to_all.16 = bf16[4,64,2048]{2,1,0:T(8,128)(2,1)S(1)} all-to-all(bf16[4,64,2048]{2,1,0:T(8,128)(2,1)S(1)} %bitcast.618), channel_id=1, replica_groups=mesh['sp_0'=16,'sp_1'=4,'sp_2'=2,'tp'=4] {'tp'}, dimensions={0} | all-to-all | bytes 2097152 | tf_op jit(solution)/shard_map/all_to_all | solution.py:121
  (498 shorter events, 127.7 us)
Async XLA Ops:
  6.5 19.8 %copy-start = (bf16[2,2048,8]{1,2,0:T(8,128)(2,1)S(1)}, bf16[2,2048,8]{1,2,0:T(8,128)(2,1)}, u32[]{:S(2)}) copy-start(bf16[2,2048,8]{1,2,0:T(8,128)(2,1)} %param.27) | copy-start | bytes 196612
  6.5 11.0 %copy-start.97 = (f32[2,8]{1,0:T(2,128)S(1)}, f32[2,8]{1,0:T(2,128)}, u32[]{:S(2)}) copy-start(f32[2,8]{1,0:T(2,128)} %param.28) | copy-start | bytes 196
  6.5 151.1 %all-gather.20.cloned.1.call-start = ((), (), s32[]{:S(2)}) async-start(), calls=%async_computation.3 | async-start | bytes 3170304 | tf_op jit(solution)/shard_map/all_gather | solution.py:42
  10.0 14.8 %all-to-all-start = ((bf16[4,256,512]{2,1,0:T(8,128)(2,1)}), bf16[4,256,512]{2,1,0:T(8,128)(2,1)S(1)}, u32[]{:S(2)}, u32[]{:S(2)}) async-start(bf16[4,256,512]{2,1,0:T(8,128)(2,1)} %broadcast_in_dim.174), calls=%async_computation | async-start | bytes 2097152 | tf_op jit(solution)/shard_map/all_to_all | solution.py:22
  15.0 345.4 %all-gather.24.cloned.1.call-start = ((), (), s32[]{:S(2)}) async-start(), calls=%async_computation.5 | async-start | bytes 2113536 | tf_op jit(solution)/shard_map/all_gather | solution.py:42
  15.7 373.2 %all-gather.30.cloned.1.call-start = ((), (), s32[]{:S(2)}) async-start(), calls=%async_computation.8 | async-start | bytes 1114112 | tf_op jit(solution)/shard_map/all_gather | solution.py:57
  28.3 131.9 %copy-start.63 = (f32[2,4,64]{2,1,0:T(4,128)}, f32[2,4,64]{2,1,0:T(4,128)S(1)}, u32[]{:S(2)}) copy-start(f32[2,4,64]{2,1,0:T(4,128)S(1)} %mul.661) | copy-start | bytes 6148
  28.5 143.4 %copy-start.61 = (f32[2,4,64]{2,1,0:T(4,128)}, f32[2,4,64]{2,1,0:T(4,128)S(1)}, u32[]{:S(2)}) copy-start(f32[2,4,64]{2,1,0:T(4,128)S(1)} %mul.643) | copy-start | bytes 6148
  243.9 11.0 %copy-start.46 = (f32[4,2,64,128]{3,2,0,1:T(8,128)}, f32[4,2,64,128]{3,2,0,1:T(8,128)S(1)}, u32[]{:S(2)}) copy-start(f32[4,2,64,128]{3,2,0,1:T(8,128)S(1)} %get-tuple-element.102) | copy-start | bytes 786436
  281.3 12.7 %copy-start.36 = (f32[2,4,8,1,4,4]{5,3,2,4,1,0:T(1,128)S(1)}, f32[2,4,8,1,4,4]{5,3,2,4,1,0:T(1,128)}, u32[]{:S(2)}) copy-start(f32[2,4,8,1,4,4]{5,3,2,4,1,0:T(1,128)} %copy-done.35) | copy-start | bytes 12292
  281.4 14.2 %copy-start.24 = (f32[2,4,8,1,4,4]{5,3,2,4,1,0:T(1,128)S(1)}, f32[2,4,8,1,4,4]{5,3,2,4,1,0:T(1,128)}, u32[]{:S(2)}) copy-start(f32[2,4,8,1,4,4]{5,3,2,4,1,0:T(1,128)} %copy-done.23) | copy-start | bytes 12292
  281.9 15.3 %copy-start.50 = (f32[4,2,4,16,16]{4,3,0,2,1:T(8,128)S(1)}, f32[4,2,4,16,16]{4,3,0,2,1:T(8,128)}, u32[]{:S(2)}) copy-start(f32[4,2,4,16,16]{4,3,0,2,1:T(8,128)} %copy.547) | copy-start | bytes 98308
  299.4 11.9 %copy-start.29 = (f32[2,128,128]{2,1,0:T(8,128)}, f32[2,128,128]{2,1,0:T(8,128)S(1)}, u32[]{:S(2)}) copy-start(f32[2,128,128]{2,1,0:T(8,128)S(1)} %convolution_add_fusion.26) | copy-start | bytes 393220
  299.7 11.7 %copy-start.31 = (f32[2,128,128]{2,1,0:T(8,128)}, f32[2,128,128]{2,1,0:T(8,128)S(1)}, u32[]{:S(2)}) copy-start(f32[2,128,128]{2,1,0:T(8,128)S(1)} %fusion.226) | copy-start | bytes 393220
  299.7 12.4 %copy-start.43 = (f32[2,256,128]{2,1,0:T(8,128)S(1)}, f32[2,256,128]{2,1,0:T(8,128)}, u32[]{:S(2)}) copy-start(f32[2,256,128]{2,1,0:T(8,128)} %copy.405) | copy-start | bytes 786436
  299.7 12.4 %copy-start.62 = (f32[2,4,64]{2,1,0:T(4,128)S(1)}, f32[2,4,64]{2,1,0:T(4,128)}, u32[]{:S(2)}) copy-start(f32[2,4,64]{2,1,0:T(4,128)} %copy-done.61) | copy-start | bytes 6148
  299.9 12.7 %copy-start.25 = (f32[2,128,128]{2,1,0:T(8,128)}, f32[2,128,128]{2,1,0:T(8,128)S(1)}, u32[]{:S(2)}) copy-start(f32[2,128,128]{2,1,0:T(8,128)S(1)} %fusion.325) | copy-start | bytes 393220
  300.1 11.5 %copy-start.33 = (f32[2,128,128]{2,1,0:T(8,128)}, f32[2,128,128]{2,1,0:T(8,128)S(1)}, u32[]{:S(2)}) copy-start(f32[2,128,128]{2,1,0:T(8,128)S(1)} %fusion.326) | copy-start | bytes 393220
  301.9 128.1 %all-gather.32.cloned.1.call-start = ((), (), s32[]{:S(2)}) async-start(), calls=%async_computation.9 | async-start | bytes 1114112 | tf_op jit(solution)/shard_map/all_gather | solution.py:57
  316.0 183.7 %all-gather.26.cloned.1.call-start = ((), (), s32[]{:S(2)}) async-start(), calls=%async_computation.6 | async-start | bytes 1114112 | tf_op jit(solution)/shard_map/all_gather | solution.py:57
  323.2 25.2 %copy-start.49 = (f32[4,2,64,128]{3,2,0,1:T(8,128)}, f32[4,2,64,128]{3,2,0,1:T(8,128)S(1)}, u32[]{:S(2)}) copy-start(f32[4,2,64,128]{3,2,0,1:T(8,128)S(1)} %get-tuple-element.98) | copy-start | bytes 786436
  342.0 17.8 %copy-start.66 = (bf16[31,256]{1,0:T(8,128)(2,1)S(1)}, bf16[31,256]{1,0:T(8,128)(2,1)}, u32[]{:S(2)}) copy-start(bf16[31,256]{1,0:T(8,128)(2,1)} %param.34) | copy-start | bytes 47620
  342.9 226.5 %all-gather.28.cloned.1.call-start = ((), (), s32[]{:S(2)}) async-start(), calls=%async_computation.7 | async-start | bytes 1114112 | tf_op jit(solution)/shard_map/all_gather | solution.py:57
  362.3 8.7 %copy-start.87 = (f32[1,256]{1,0:T(1,128)S(1)}, f32[1,256]{1,0:T(1,128)}, u32[]{:S(2)}) copy-start(f32[1,256]{1,0:T(1,128)} %get-tuple-element.340) | copy-start | bytes 3076
  362.3 8.7 %copy-start.88 = (f32[1,256]{1,0:T(1,128)S(1)}, f32[1,256]{1,0:T(1,128)}, u32[]{:S(2)}) copy-start(f32[1,256]{1,0:T(1,128)} %get-tuple-element.341) | copy-start | bytes 3076
  362.3 8.7 %copy-start.89 = (f32[1,256]{1,0:T(1,128)S(1)}, f32[1,256]{1,0:T(1,128)}, u32[]{:S(2)}) copy-start(f32[1,256]{1,0:T(1,128)} %get-tuple-element.342) | copy-start | bytes 3076
  362.3 8.7 %copy-start.90 = (f32[1,256]{1,0:T(1,128)S(1)}, f32[1,256]{1,0:T(1,128)}, u32[]{:S(2)}) copy-start(f32[1,256]{1,0:T(1,128)} %get-tuple-element.343) | copy-start | bytes 3076
  362.3 8.7 %copy-start.91 = (f32[1,256]{1,0:T(1,128)S(1)}, f32[1,256]{1,0:T(1,128)}, u32[]{:S(2)}) copy-start(f32[1,256]{1,0:T(1,128)} %get-tuple-element.344) | copy-start | bytes 3076
  362.3 8.7 %copy-start.92 = (f32[1,256]{1,0:T(1,128)S(1)}, f32[1,256]{1,0:T(1,128)}, u32[]{:S(2)}) copy-start(f32[1,256]{1,0:T(1,128)} %get-tuple-element.345) | copy-start | bytes 3076
  362.4 8.7 %copy-start.93 = (f32[1,256]{1,0:T(1,128)S(1)}, f32[1,256]{1,0:T(1,128)}, u32[]{:S(2)}) copy-start(f32[1,256]{1,0:T(1,128)} %get-tuple-element.346) | copy-start | bytes 3076
  362.4 14.5 %copy-start.79 = (bf16[256,16]{0,1:T(8,128)(2,1)S(1)}, bf16[256,16]{0,1:T(8,128)(2,1)}, u32[]{:S(2)}) copy-start(bf16[256,16]{0,1:T(8,128)(2,1)} %param.37) | copy-start | bytes 24580
  362.4 14.5 %copy-start.80 = (bf16[256,16]{0,1:T(8,128)(2,1)S(1)}, bf16[256,16]{0,1:T(8,128)(2,1)}, u32[]{:S(2)}) copy-start(bf16[256,16]{0,1:T(8,128)(2,1)} %param.36) | copy-start | bytes 24580
  362.4 18.7 %copy-start.12 = (f32[2,4,64,64]{3,2,1,0:T(8,128)S(1)}, f32[2,4,64,64]{3,2,1,0:T(8,128)}, u32[]{:S(2)}) copy-start(f32[2,4,64,64]{3,2,1,0:T(8,128)} %convolution_multiply_fusion) | copy-start | bytes 393220
  362.4 18.7 %copy-start.14 = (f32[2,4,64,128]{3,2,1,0:T(8,128)S(1)}, f32[2,4,64,128]{3,2,1,0:T(8,128)}, u32[]{:S(2)}) copy-start(f32[2,4,64,128]{3,2,1,0:T(8,128)} %copy-done.13) | copy-start | bytes 786436
  362.4 21.9 %copy-start.16 = (f32[2,4,64,128]{3,2,1,0:T(8,128)S(1)}, f32[2,4,64,128]{3,2,1,0:T(8,128)}, u32[]{:S(2)}) copy-start(f32[2,4,64,128]{3,2,1,0:T(8,128)} %copy-done.15) | copy-start | bytes 786436
  362.4 21.9 %copy-start.18 = (f32[2,4,64,64]{3,2,1,0:T(8,128)S(1)}, f32[2,4,64,64]{3,2,1,0:T(8,128)}, u32[]{:S(2)}) copy-start(f32[2,4,64,64]{3,2,1,0:T(8,128)} %convolution_multiply_fusion.2) | copy-start | bytes 393220
  362.9 22.9 %copy-start.22 = (f32[2,128,128]{2,1,0:T(8,128)S(1)}, f32[2,128,128]{2,1,0:T(8,128)}, u32[]{:S(2)}) copy-start(f32[2,128,128]{2,1,0:T(8,128)} %copy-done.21) | copy-start | bytes 393220
  363.0 7.1 collective-permute-start.1
  367.9 3.1 collective-permute-start
  371.0 15.1 %copy-start.28 = (f32[2,128,128]{2,1,0:T(8,128)S(1)}, f32[2,128,128]{2,1,0:T(8,128)}, u32[]{:S(2)}) copy-start(f32[2,128,128]{2,1,0:T(8,128)} %copy-done.27) | copy-start | bytes 393220
  371.0 15.1 %copy-start.38 = (f32[2,128,128]{2,1,0:T(8,128)S(1)}, f32[2,128,128]{2,1,0:T(8,128)}, u32[]{:S(2)}) copy-start(f32[2,128,128]{2,1,0:T(8,128)} %copy-done.37) | copy-start | bytes 393220
  371.0 15.1 %copy-start.40 = (f32[2,128,128]{2,1,0:T(8,128)S(1)}, f32[2,128,128]{2,1,0:T(8,128)}, u32[]{:S(2)}) copy-start(f32[2,128,128]{2,1,0:T(8,128)} %copy-done.39) | copy-start | bytes 393220
  372.9 8.2 %all-to-all-start.1 = ((f32[4,1,512]{2,1,0:T(1,128)}), f32[4,1,512]{2,1,0:T(1,128)S(1)}, u32[]{:S(2)}, u32[]{:S(2)}) async-start(f32[4,1,512]{2,1,0:T(1,128)} %broadcast_in_dim.178), calls=%async_computation.1 | async-start | bytes 16384 | tf_op jit(solution)/shard_map/all_to_all | solution.py:22
  376.9 344.1 %all-gather.22.cloned.1.call-start = ((), (), s32[]{:S(2)}) async-start(), calls=%async_computation.4 | async-start | bytes 2113536 | tf_op jit(solution)/shard_map/all_gather | solution.py:105
  388.9 46.6 %copy-start.3 = (bf16[32,128,128]{2,1,0:T(8,128)(2,1)S(1)}, bf16[32,128,128]{2,1,0:T(8,128)(2,1)}, u32[]{:S(2)}) copy-start(bf16[32,128,128]{2,1,0:T(8,128)(2,1)} %all-gather.30.cloned.1.call-done) | copy-start | bytes 3145732
  499.7 74.3 %copy-start.4 = (bf16[32,128,128]{2,1,0:T(8,128)(2,1)S(1)}, bf16[32,128,128]{2,1,0:T(8,128)(2,1)}, u32[]{:S(2)}) copy-start(bf16[32,128,128]{2,1,0:T(8,128)(2,1)} %all-gather.26.cloned.1.call-done) | copy-start | bytes 3145732
  588.0 134.9 %copy-start.96 = (f32[256]{0:T(256)S(1)}, f32[256]{0:T(256)}, u32[]{:S(2)}) copy-start(f32[256]{0:T(256)} %param.35) | copy-start | bytes 3076
  722.9 19.9 %copy-start.1 = (bf16[2,2048,8]{1,2,0:T(8,128)(2,1)S(1)}, bf16[2,2048,8]{1,2,0:T(8,128)(2,1)}, u32[]{:S(2)}) copy-start(bf16[2,2048,8]{1,2,0:T(8,128)(2,1)} %param.27) | copy-start | bytes 196612
  (62 other events, 264.2 us)
Sparse Core Ops, SparseCore 0:
  10.5 147.1 all-gather.19
  160.8 136.9 all-gather.23
  302.1 58.5 all-gather.29
  362.6 67.4 all-gather.31
  432.0 67.6 all-gather.25
  501.6 67.6 all-gather.27
  572.5 148.4 all-gather.21
where the time goes:
time: 759 us; the launch traced here: 750 us
  waiting for transfers between devices  441 us (58%)
  local copies, waits for them, and re-layouts  97 us (13%)
  matrix products  89.5 us (12%)
  blocking collectives  72.7 us (10%)
  between operations  16.6 us (2%)
  other arithmetic  16.4 us (2%)
  starting transfers between devices  16.3 us (2%)
    all_gather x4, waiting for transfers between devices, prefix_by_axis(): lax.all_gather(part.astype(kind), axis)  171 us
    all_gather x1, waiting for transfers between devices, gather_turned(): out, at, gathered = (lax.all_gather(both, axis, axis=0, tiled=True), 0, [])  133 us
    all_gather x2, waiting for transfers between devices, side_by_side(): lax.all_gather(both, axis, axis=dim, tiled=True)  125 us
    dot_general x136, matrix products, matmul_high(): return jnp.matmul(left_side, right_side, precision=highest)  78.2 us
    all_gather x8, blocking collectives, prefix_by_axis(): lax.all_gather(part.astype(kind), axis)  54.2 us
    reshape x18, local copies, waits for them, and re-layouts, unit_lower_inverse(): matrix.reshape(leading + (pair_count, 2 * size_now, pair_count, 2 * size_...  49.4 us
    gather x18, local copies, waits for them, and re-layouts, unit_lower_inverse(): jnp.diagonal(block_grid, axis1=-4, axis2=-2)  22.5 us
    all_to_all x1, blocking collectives, sent_and_summed(): lax.all_to_all(tiles, axis, split_axis=0, concat_axis=0, tiled=True)  18.4 us
  transfers between devices with their start and end apart: 11, of which 8 were waited for; matrix products, arithmetic and copies ran while one was open for 26% of the time, Pallas kernels for 0%

commit v1 on v0

v1 whole, which is shorter than its diff:
```python
import jax
import jax.numpy as jnp
from jax import lax
from jax.experimental import pallas as pl
from jax.experimental.pallas import tpu as pltpu
from jax.sharding import Mesh
from jax.sharding import PartitionSpec as P

HEAD = 128
V_HEADS = 8
CONV_CH = 1024
KERNEL = 31
SP = ("sp_0", "sp_1", "sp_2")
SP_TP = ("sp_0", "sp_1", "sp_2", "tp")
Z, X, C, Y = (16, 4, 2, 4)
ROWS = 256
WIDE = 256
F32 = jnp.float32
BF16 = jnp.bfloat16
HIGHEST = lax.Precision.HIGHEST
MESH = pl.DeviceIdType.MESH
VMEM = pl.BlockSpec(memory_space=pltpu.VMEM)
PACKET = 208


def place():
    return tuple(lax.axis_index(a) for a in SP_TP)


def remote(src, dst, send, recv, to):
    return pltpu.make_async_remote_copy(
        src_ref=src, dst_ref=dst, send_sem=send, recv_sem=recv, device_id=to, device_id_type=MESH
    )


def greet(peers):
    barrier = pltpu.get_barrier_semaphore()
    for peer in peers:
        pl.semaphore_signal(barrier, inc=1, device_id=peer, device_id_type=MESH)
    pl.semaphore_wait(barrier, len(peers))


def bdot(a, b, dims):
    return lax.dot_general(
        a.astype(BF16), b.astype(BF16), (dims, ((), ())), preferred_element_type=F32
    )


def fdot(a, b, dims):
    return lax.dot_general(a, b, (dims, ((), ())), precision=HIGHEST, preferred_element_type=F32)


def gather_kernel(w_ref, x_ref, g_ref, f_ref, zs, zr, xs, xr, ds, dr, ys, yr, own):
    z, x, c, y = place()
    zp, zm = (lax.rem(z + 1, Z), lax.rem(z + Z - 1, Z))
    xp, xm = (lax.rem(x + 1, X), lax.rem(x + X - 1, X))
    up, down = ((zp, x, c, y), (zm, x, c, y))
    right, left = ((z, xp, c, y), (z, xm, c, y))
    other = (z, x, 1 - c, y)
    mates = [(z, x, c, lax.rem(y + d, Y)) for d in (2, 1, 3)]

    greet([up, down, right, left, other] + mates)

    feature_copies = []
    for i, mate in enumerate(mates):
        copy = remote(x_ref, f_ref.at[y], ys.at[i], yr.at[i], mate)
        copy.start()
        feature_copies.append(copy)

    def chunk(zi, xi):
        return g_ref.at[:, zi, xi, c]

    def z_copy(src, zi, s, way, to):
        return remote(src, chunk(zi, x), zs.at[s, way], zr.at[s, way], to)

    def x_copy(src, zi, xi, s, way, to):
        return remote(src, chunk(zi, xi), xs.at[s, way], xr.at[s, way], to)

    def d_copy(zi, ci, s, way):
        line = g_ref.at[:, zi, :, ci]
        return remote(line, line, ds.at[s, way], dr.at[s, way], other)

    def behind(s):
        return lax.rem(z + Z - s, Z)

    def ahead(s):
        return lax.rem(z + s, Z)

    def z_start(s):
        p = chunk(behind(s), x)
        z_copy(p, behind(s), s, 0, up).wait_recv()

    def spread_p(s, src):
        x_copy(src, behind(s), x, s, 0, right).start()
        x_copy(src, behind(s), x, s, 1, left).start()

    def spread_q(s):
        src = chunk(ahead(s), x)
        x_copy(src, ahead(s), x, s, 2, left).start()
        x_copy(src, ahead(s), x, s, 3, right).start()

    def along_z(s, both, go_p, go_q):
        p, q = (chunk(behind(s), x), chunk(ahead(s), x))
        z_copy(p, behind(s), s, 0, up).wait_recv()
        if go_p:
            z_copy(p, behind(s), s + 1, 0, up).start()
        if both:
            z_copy(q, ahead(s), s, 1, down).wait_recv()
            if go_q:
                z_copy(q, ahead(s), s + 1, 1, down).start()
        spread_p(s, p)
        if both:
            spread_q(s)

    def forward(s, both):
        p = chunk(behind(s), xm)
        x_copy(p, behind(s), xm, s, 0, right).wait_recv()
        x_copy(p, behind(s), xm, s, 4, right).start()
        if both:
            q = chunk(ahead(s), xp)
            x_copy(q, ahead(s), xp, s, 2, left).wait_recv()
            x_copy(q, ahead(s), xp, s, 5, left).start()

    def across(s, both):
        far = lax.rem(x + 2, X)
        x_copy(chunk(behind(s), xp), behind(s), xp, s, 1, left).wait_recv()
        x_copy(chunk(behind(s), far), behind(s), far, s, 4, right).wait_recv()
        d_copy(behind(s), c, s, 0).start()
        if both:
            x_copy(chunk(ahead(s), xm), ahead(s), xm, s, 3, right).wait_recv()
            x_copy(chunk(ahead(s), far), ahead(s), far, s, 5, left).wait_recv()
            d_copy(ahead(s), c, s, 1).start()

    z_copy(w_ref, z, 1, 0, up).start()
    z_copy(w_ref, z, 1, 1, down).start()
    spread_p(0, w_ref)
    mine = pltpu.make_async_copy(w_ref, chunk(z, x), own.at[0])
    mine.start()
    keep = pltpu.make_async_copy(x_ref, f_ref.at[y], own.at[1])
    keep.start()
    mine.wait()
    along_z(1, True, True, True)
    forward(0, False)
    along_z(2, True, True, True)
    forward(1, True)
    across(0, False)

    @pl.loop(3, 7)
    def _(s):
        along_z(s, True, True, True)
        forward(s - 1, True)
        across(s - 2, True)

    along_z(7, True, True, False)
    forward(6, True)
    across(5, True)
    along_z(8, False, False, False)
    forward(7, True)
    across(6, True)
    forward(8, False)
    across(7, True)
    across(8, False)

    def d_arrived(s, way):
        d_copy(behind(s) if way == 0 else ahead(s), 1 - c, s, way).wait_recv()

    def sent(s, both, zed):
        p, q = (chunk(behind(s), x), chunk(ahead(s), x))
        if zed:
            z_copy(p, behind(s), s, 0, up).wait_send()
            if both:
                z_copy(q, ahead(s), s, 1, down).wait_send()
        for way in (0, 1, 4) + ((2, 3, 5) if both else ()):
            x_copy(p, behind(s), x, s, way, right).wait_send()
        d_copy(behind(s), c, s, 0).wait_send()
        if both:
            d_copy(ahead(s), c, s, 1).wait_send()

    d_arrived(0, 0)
    sent(0, False, False)

    @pl.loop(1, 8)
    def _(s):
        d_arrived(s, 0)
        d_arrived(s, 1)
        sent(s, True, True)

    d_arrived(8, 0)
    sent(8, False, True)
    for i, copy in enumerate(feature_copies):
        copy.wait_send()
    for i, mate in enumerate(mates):
        src_y = lax.rem(y + Y - (2, 1, 3)[i], Y)
        remote(x_ref, f_ref.at[src_y], ys.at[i], yr.at[i], mate).wait_recv()
    keep.wait()


def gather_call(packed, features):
    count = packed.shape[0]
    dma = pltpu.SemaphoreType.DMA
    return pl.pallas_call(
        gather_kernel,
        out_shape=(
            jax.ShapeDtypeStruct((count, Z, X, C, 16, WIDE), BF16),
            jax.ShapeDtypeStruct((Y, ROWS, 512), BF16),
        ),
        in_specs=[VMEM] * 2,
        out_specs=(VMEM, VMEM),
        scratch_shapes=[
            dma((9, 2)), dma((9, 2)), dma((9, 6)), dma((9, 6)), dma((9, 2)), dma((9, 2)),
            dma((3,)), dma((3,)), dma((2,)),
        ],
        compiler_params=pltpu.CompilerParams(
            collective_id=0, has_side_effects=True, vmem_limit_bytes=40 * 2**20
        ),
        name="gather",
    )(packed, features)


def triangle(lower, strict):
    i = lax.broadcasted_iota(jnp.int32, (ROWS, ROWS), 0)
    j = lax.broadcasted_iota(jnp.int32, (ROWS, ROWS), 1)
    if lower:
        return i > j if strict else i >= j
    return i < j if strict else i <= j


def unit_inverse(below):
    i = lax.broadcasted_iota(jnp.int32, (ROWS, ROWS), 0)
    j = lax.broadcasted_iota(jnp.int32, (ROWS, ROWS), 1)
    eye = (i == j).astype(F32)
    size = 1
    inverse = None
    while size < ROWS:
        twice = 2 * size
        pair = ((i & -twice) == (j & -twice)) & ((i & size) != (j & size))
        corner = jnp.where(pair, below, 0.0)
        if inverse is None:
            inverse = eye - corner
        else:
            inner = bdot(corner, inverse, ((1,), (0,)))
            inverse = inverse - bdot(inverse, inner, ((1,), (0,)))
        size = twice
    low = (inverse - inverse.astype(BF16).astype(F32)).astype(BF16)
    high = inverse.astype(BF16)
    b_high = below.astype(BF16)
    b_low = (below - b_high.astype(F32)).astype(BF16)
    product = (
        bdot(b_high, high, ((1,), (0,)))
        + bdot(b_high, low, ((1,), (0,)))
        + bdot(b_low, high, ((1,), (0,)))
    )
    residual = eye - inverse - product
    return inverse + bdot(inverse, residual, ((1,), (0,)))


def silu(v):
    return v * jax.nn.sigmoid(v)


def local_kernel(
    f_ref, gain_ref, w_ref, gate_ref, shift_ref, pace_ref, jolt_ref,
    packet_ref, reach_ref, offset_ref, gated_ref, normed,
):
    total = jnp.zeros((ROWS, 1), F32)
    for p in range(Y):
        total = total + jnp.sum(f_ref[p].astype(F32), axis=1, keepdims=True)
    mean = total / 2048.0
    total = jnp.zeros((ROWS, 1), F32)
    for p in range(Y):
        total = total + jnp.sum(jnp.square(f_ref[p].astype(F32) - mean), axis=1, keepdims=True)
    scale = lax.rsqrt(total / 2048.0 + 1e-05)
    for p in range(Y):
        normed[:, p * 512 : (p + 1) * 512] = (
            (f_ref[p].astype(F32) - mean) * scale * gain_ref[p]
        ).astype(BF16)
    rows = normed[...]

    def project(k):
        return bdot(rows, w_ref[k], ((1,), (0,))).astype(BF16).astype(F32)

    gated_ref[...] = (project(3) * jax.nn.sigmoid(project(4))).astype(BF16)
    gates = bdot(gate_ref[...], rows, ((1,), (1,)))
    beta = jax.nn.sigmoid(gates[0:4] + shift_ref[...])
    pre = gates[4:8]
    soft = jnp.maximum(pre, 0.0) + jnp.log1p(jnp.exp(-jnp.abs(pre)))
    log_decay = -pace_ref[...] * soft + jolt_ref[...]
    upto = triangle(False, False).astype(F32)
    since = triangle(True, False).astype(F32)
    padded = jnp.concatenate([log_decay, jnp.zeros((4, ROWS), F32)], axis=0)
    ahead = fdot(padded, upto, ((1,), (0,)))
    back = fdot(padded, since, ((1,), (0,)))
    cumulative = jnp.concatenate([ahead[0:2], back[2:4]], axis=0)
    lines = jnp.concatenate([beta, cumulative], axis=0)
    columns = jnp.transpose(lines)

    query_all, key_all, value_all = (project(0), project(1), project(2))
    for h in range(2):
        lanes = slice(h * HEAD, (h + 1) * HEAD)
        q = silu(query_all[:, lanes])
        k = silu(key_all[:, lanes])
        k = k * lax.rsqrt(jnp.sum(jnp.square(k), axis=1, keepdims=True) + 1e-06)
        v = value_all[:, lanes]
        kk = bdot(k, k, ((1,), (1,)))
        qk = bdot(q, k, ((1,), (1,)))
        within = jnp.zeros((ROWS, HEAD), F32)
        for e in range(2):
            n = e * 2 + h
            b_col = columns[:, n : n + 1]
            c_col = columns[:, 4 + n : 5 + n]
            c_row = cumulative[n : n + 1, :]
            mask = triangle(e == 0, False)
            gap = jnp.where(mask, jnp.exp(jnp.where(mask, c_col - c_row, 0.0)), 0.0)
            below = jnp.where(triangle(e == 0, True), b_col * kk * gap, 0.0)
            inverse = unit_inverse(below)
            grown = jnp.exp(c_col)
            right = jnp.concatenate([v * b_col, k * (b_col * grown)], axis=1)
            both = bdot(inverse, right, ((1,), (0,)))
            read = bdot(qk * gap, both, ((1,), (0,)))
            within = within + read[:, :HEAD]
            reach_ref[e, h] = (q * grown - read[:, HEAD:]).astype(BF16)
            last = c_row[:, ROWS - 1 : ROWS] if e == 0 else c_row[:, 0:1]
            tail = k * jnp.exp(last - c_col)
            maps = bdot(both, tail, ((0,), (0,)))
            whole = jnp.broadcast_to(jnp.exp(last), (8, HEAD))
            high = whole.astype(BF16)
            low = (whole - high.astype(F32)).astype(BF16)
            for half in range(2):
                packet_ref[e, h, half, 0:128] = maps[128:256].astype(BF16)
                packet_ref[e, h, half, 128:192] = maps[half * 64 : half * 64 + 64].astype(BF16)
                packet_ref[e, h, half, 192:208] = jnp.concatenate(
                    [high.astype(F32), low.astype(F32)], axis=0
                ).astype(BF16)
        offset_ref[h] = within


def local_call(features, gain, weights, gates, shift, pace, jolt):
    return pl.pallas_call(
        local_kernel,
        out_shape=(
            jax.ShapeDtypeStruct((2, 2, 2, PACKET, HEAD), BF16),
            jax.ShapeDtypeStruct((2, 2, ROWS, HEAD), BF16),
            jax.ShapeDtypeStruct((2, ROWS, HEAD), F32),
            jax.ShapeDtypeStruct((ROWS, WIDE), BF16),
        ),
        in_specs=[VMEM] * 7,
        out_specs=(VMEM,) * 4,
        scratch_shapes=[pltpu.VMEM((ROWS, 2048), BF16)],
        compiler_params=pltpu.CompilerParams(vmem_limit_bytes=40 * 2**20),
        name="local",
    )(features, gain, weights, gates, shift, pace, jolt)


def unpack(ref, at):
    body = ref[at].astype(F32)
    return (body[0:192], body[192:193] + body[200:201])


def joined(first, second):
    (body1, a1), (body2, a2) = (first, second)
    turned = bdot(body1, body2[0:128], ((1,), (0,)))
    top = a1 * body2[0:128] + a2 * body1[0:128] - turned[0:128]
    bottom = a2 * body1[128:192] - turned[128:192] + body2[128:192]
    return (jnp.concatenate([top, bottom], axis=0), a1 * a2)


def carried_kernel(
    packet_ref, gated_ref, taps_ref, gain_ref, entry_ref, conv_ref,
    slab, before, leaving, near, far, parting, halo, stats, line, wide, filtered,
    ss, sr, ns, nr, fs, fr, es, er, hs, hr, ts, tr,
):
    z, x, c, y = place()
    step = 1 - 2 * c
    owner = c * X + x
    position = z * 8 + x * 2 + c
    mine = x * 2 + c

    def slab_peer(dx, dc):
        return (z, lax.rem(x + dx, X), c if dc == 0 else 1 - c, y)

    offsets = [(dx, dc) for dx in range(X) for dc in range(C) if (dx, dc) != (0, 0)]
    offsets = sorted(offsets, key=lambda o: -(2 if o[0] == 2 else min(o[0], 1)))
    mates = [(z, x, c, lax.rem(y + d, Y)) for d in (2, 1, 3)]

    def at_position(s):
        s = lax.rem(s + 128, 128)
        return (s // 8, lax.rem(s // 2, X), lax.rem(s, 2), y)

    following, preceding = (at_position(position + 1), at_position(position - 1))
    rest_of_z = [(lax.rem(z + d, Z), x, c, y) for d in range(1, Z)]

    near[...] = jnp.zeros_like(near)
    far[...] = jnp.zeros_like(far)
    greet([slab_peer(*o) for o in offsets] + mates + [following, preceding] + rest_of_z)

    slab_copies = []
    for i, (dx, dc) in enumerate(offsets):
        to = slab_peer(dx, dc)
        copy = remote(
            packet_ref.at[to[2] * X + to[1]], slab.at[mine], ss.at[i], sr.at[i], to
        )
        copy.start()
        slab_copies.append(copy)
    halo_copies = [
        remote(gated_ref.at[ROWS - 16 : ROWS], halo.at[0], hs.at[0], hr.at[0], following),
        remote(gated_ref.at[0:16], halo.at[1], hs.at[1], hr.at[1], preceding),
    ]
    for copy in halo_copies:
        copy.start()
    slab[mine] = packet_ref[owner]

    wide[16 : 16 + ROWS] = gated_ref[...].astype(F32)
    for copy in halo_copies:
        copy.wait_recv()
    wide[0:16] = halo[0].astype(F32) * (position > 0).astype(F32)
    wide[16 + ROWS : 32 + ROWS] = halo[1].astype(F32) * (position < 127).astype(F32)
    taps = taps_ref[...].astype(F32)

    @pl.loop(0, ROWS // 32)
    def _(r):
        window = wide[pl.ds(pl.multiple_of(r * 32, 32), 64)]
        total = jnp.zeros((32, WIDE), F32)
        for j in range(KERNEL):
            total = total + window[j + 1 : j + 33] * taps[j : j + 1]
        filtered[pl.ds(pl.multiple_of(r * 32, 32), 32)] = total

    ones = jnp.ones((8, WIDE), F32)
    whole = filtered[...]
    line[0:8] = fdot(ones, whole, ((1,), (1,)))
    line[8:16] = fdot(ones, whole * whole, ((1,), (1,)))
    stat_copies = []
    for i, mate in enumerate(mates):
        copy = remote(line, stats.at[i], ts.at[i], tr.at[i], mate)
        copy.start()
        stat_copies.append(copy)

    for i, (dx, dc) in enumerate(offsets):
        source = slab_peer(X - dx, dc)
        remote(
            packet_ref.at[owner], slab.at[source[1] * 2 + source[2]], ss.at[i], sr.at[i], source
        ).wait_recv()

    def nth(t):
        return jnp.where(c == 0, t, 7 - t)

    running = unpack(slab, nth(0))
    for t in range(1, 8):
        before[t, 0:192] = running[0].astype(BF16)
        before[t, 192:208] = jnp.broadcast_to(running[1], (16, HEAD)).astype(BF16)
        parting[t] = running[1]
        running = joined(running, unpack(slab, nth(t)))

    def pack(ref, value):
        body, a = value
        high = a.astype(BF16).astype(F32)
        ref[0:192] = body.astype(BF16)
        ref[192:208] = jnp.concatenate(
            [jnp.broadcast_to(high, (8, HEAD)), jnp.broadcast_to(a - high, (8, HEAD))], axis=0
        ).astype(BF16)

    def hop(d):
        return z + step * d

    def inside(d):
        return (hop(d) >= 0) & (hop(d) < Z)

    def z_peer(d):
        return (jnp.clip(hop(d), 0, Z - 1), x, c, y)

    def near_copy(i, d):
        return remote(leaving.at[0], near.at[i], ns.at[i], nr.at[i], z_peer(d))

    def far_copy(i, d):
        return remote(leaving.at[1], far.at[i], fs.at[i], fr.at[i], z_peer(d))

    pack(leaving.at[0], running)
    for i, d in ((2, 3), (1, 2), (0, 1)):

        @pl.when(inside(d))
        def _():
            near_copy(i, d).start()

    for copy in stat_copies:
        copy.wait_recv()
    summed = line[...] + stats[0] + stats[1] + stats[2]
    spread = jnp.full((8, WIDE), 0.125, F32)
    mean = fdot(summed[0:8], spread, ((0,), (0,))) / CONV_CH
    second = fdot(summed[8:16], spread, ((0,), (0,))) / CONV_CH
    conv_ref[...] = silu(
        (filtered[...] - mean) * lax.rsqrt(second - mean * mean + 1e-05) * gain_ref[...]
    ).astype(BF16)

    window = running
    for i, d in ((0, 1), (1, 2), (2, 3)):

        @pl.when(inside(-d))
        def _():
            near_copy(i, d).wait_recv()

        window = joined(unpack(near, i), window)
    pack(leaving.at[1], window)
    reaches = ((2, 9), (1, 5), (3, 13), (0, 1))
    for i, d in reaches:

        @pl.when(inside(d))
        def _():
            far_copy(i, d).start()

    @pl.when(inside(-1))
    def _():
        far_copy(0, 1).wait_recv()

    entering = unpack(far, 0)
    for i, d in ((1, 5), (2, 9), (3, 13)):

        @pl.when(inside(-d))
        def _():
            far_copy(i, d).wait_recv()

        entering = joined(unpack(far, i), entering)
    state = entering[0][128:192]
    line_up = [state]
    for t in range(1, 8):
        body = before[t].astype(F32)
        line_up.append(
            parting[t] * state - bdot(state, body[0:128], ((1,), (0,))) + body[128:192]
        )
    for t in range(8):
        slab[nth(t), 0:64] = line_up[t].astype(BF16)
    entry_ref[owner] = slab[mine, 0:64]
    entry_copies = []
    for i, (dx, dc) in enumerate(offsets):
        to = slab_peer(dx, dc)
        copy = remote(
            slab.at[to[1] * 2 + to[2], 0:64], entry_ref.at[owner], es.at[i], er.at[i], to
        )
        copy.start()
        entry_copies.append(copy)
    for i, (dx, dc) in enumerate(offsets):
        source = slab_peer(X - dx, dc)
        remote(
            slab.at[0, 0:64], entry_ref.at[source[2] * X + source[1]], es.at[i], er.at[i], source
        ).wait_recv()
    for copy in slab_copies + halo_copies + stat_copies + entry_copies:
        copy.wait_send()
    for i, d in ((0, 1), (1, 2), (2, 3)):

        @pl.when(inside(d))
        def _():
            near_copy(i, d).wait_send()

    for i, d in reaches:

        @pl.when(inside(d))
        def _():
            far_copy(i, d).wait_send()


def carried_call(packets, gated, taps, gain):
    dma = pltpu.SemaphoreType.DMA
    return pl.pallas_call(
        carried_kernel,
        out_shape=(
            jax.ShapeDtypeStruct((8, 64, HEAD), BF16),
            jax.ShapeDtypeStruct((ROWS, WIDE), BF16),
        ),
        in_specs=[VMEM] * 4,
        out_specs=(VMEM, VMEM),
        scratch_shapes=[
            pltpu.VMEM((8, PACKET, HEAD), BF16),
            pltpu.VMEM((8, PACKET, HEAD), BF16),
            pltpu.VMEM((2, PACKET, HEAD), BF16),
            pltpu.VMEM((3, PACKET, HEAD), BF16),
            pltpu.VMEM((4, PACKET, HEAD), BF16),
            pltpu.VMEM((8, 1, HEAD), F32),
            pltpu.VMEM((2, 16, WIDE), BF16),
            pltpu.VMEM((3, 16, WIDE), F32),
            pltpu.VMEM((16, WIDE), F32),
            pltpu.VMEM((ROWS + 64, WIDE), F32),
            pltpu.VMEM((ROWS, WIDE), F32),
            dma((7,)), dma((7,)), dma((3,)), dma((3,)), dma((4,)), dma((4,)),
            dma((7,)), dma((7,)), dma((2,)), dma((2,)), dma((3,)), dma((3,)),
        ],
        compiler_params=pltpu.CompilerParams(
            collective_id=1, has_side_effects=True, vmem_limit_bytes=40 * 2**20
        ),
        name="carried",
    )(packets, gated, taps, gain)


def final_kernel(
    entry_ref, reach_ref, offset_ref, conv_ref, gain_ref, w_ref, out_ref, parts, landed, s, r
):
    z, x, c, y = place()
    turns = (2, 1, 3)
    greet([(z, x, c, lax.rem(y + d, Y)) for d in turns])
    heads = []
    for h in range(2):
        o = offset_ref[h]
        for e in range(2):
            at = e * 4 + h * 2
            state = jnp.concatenate([entry_ref[at], entry_ref[at + 1]], axis=0)
            o = o + bdot(reach_ref[e, h], state, ((1,), (1,)))
        scale = lax.rsqrt(jnp.mean(jnp.square(o), axis=1, keepdims=True) + 1e-06)
        heads.append((o * scale * gain_ref[...]).astype(BF16))
    left = jnp.concatenate(heads, axis=1)
    total = bdot(left, w_ref[0], ((1,), (1,))) + bdot(conv_ref[...], w_ref[1], ((1,), (1,)))
    for p in range(Y):
        parts[p] = total[p * 64 : (p + 1) * 64].astype(BF16)
    copies = []
    for i, d in enumerate(turns):
        to = lax.rem(y + d, Y)
        copy = remote(parts.at[to], landed.at[i], s.at[i], r.at[i], (z, x, c, to))
        copy.start()
        copies.append(copy)
    result = parts[y].astype(F32)
    for i in (1, 2, 0):
        copies[i].wait_recv()
        result = result + landed[i].astype(F32)
    out_ref[...] = result.astype(BF16)
    for copy in copies:
        copy.wait_send()


def final_call(entry, reach, offset, conv_out, gain, weights):
    dma = pltpu.SemaphoreType.DMA
    return pl.pallas_call(
        final_kernel,
        out_shape=jax.ShapeDtypeStruct((64, 2048), BF16),
        in_specs=[VMEM] * 6,
        out_specs=VMEM,
        scratch_shapes=[
            pltpu.VMEM((Y, 64, 2048), BF16),
            pltpu.VMEM((3, 64, 2048), BF16),
            dma((3,)),
            dma((3,)),
        ],
        compiler_params=pltpu.CompilerParams(
            collective_id=2, has_side_effects=True, vmem_limit_bytes=40 * 2**20
        ),
        name="final",
    )(entry, reach, offset, conv_out, gain, weights)


def on_device(
    inputs,
    in_gain,
    query_weight,
    key_weight,
    value_weight,
    beta_weight,
    decay_weight,
    beta_shift,
    decay_pace,
    decay_jolt,
    head_gain,
    glu_value_weight,
    glu_gate_weight,
    conv_kernel,
    conv_gain,
    out_delta_weight,
    out_conv_weight,
):
    packed = jnp.stack(
        [
            query_weight,
            key_weight,
            value_weight,
            glu_value_weight,
            glu_gate_weight,
            out_delta_weight.T,
            out_conv_weight.T,
        ]
    )
    gathered, features = gather_call(packed, inputs)
    weights = gathered.reshape(7, 2048, WIDE)
    first = lax.axis_index("tp") * 2
    gates = jnp.stack([beta_weight, decay_weight])
    gates = lax.dynamic_slice_in_dim(gates, first, 2, 3)
    gates = jnp.transpose(gates, (0, 1, 3, 2)).reshape(8, 2048)
    shift = lax.dynamic_slice_in_dim(beta_shift, first, 2, 1).reshape(4, 1)
    packets, reach, offset, gated = local_call(
        features,
        in_gain.reshape(Y, 1, 512),
        weights[:5],
        gates,
        shift,
        decay_pace.reshape(4, ROWS),
        decay_jolt.reshape(4, ROWS),
    )
    entry, conv_out = carried_call(
        packets.reshape(8, PACKET, HEAD), gated, conv_kernel, conv_gain.reshape(1, WIDE)
    )
    return final_call(entry, reach, offset, conv_out, head_gain.reshape(1, HEAD), weights[5:])


def solution(mesh):
    finer = Mesh(mesh.devices.reshape(16, 4, 2, mesh.shape["tp"]), SP_TP)
    in_specs = (
        P(SP, "tp"),
        P(),
        P(SP, "tp"),
        P(SP, "tp"),
        P(SP, "tp"),
        P(),
        P(),
        P(),
        P(None, "tp", SP),
        P(None, "tp", SP),
        P(),
        P(SP, "tp"),
        P(SP, "tp"),
        P(None, "tp"),
        P("tp"),
        P("tp", SP),
        P("tp", SP),
    )
    return jax.shard_map(
        on_device, mesh=finer, in_specs=in_specs, out_specs=P(SP_TP, None), check_vma=False
    )
```

time: 759 us -> 135 us (0.18); the launches traced: 750 us -> 135 us
  waiting for transfers between devices: 441 us -> 0 us
  Pallas kernels: 0 us -> 118 us
  matrix products: 89.5 us -> 0 us
  local copies, waits for them, and re-layouts: 97 us -> 15.6 us
  blocking collectives: 72.7 us -> 0 us
  between operations: 16.6 us -> 0.13 us
  starting transfers between devices: 16.3 us -> 0 us
  other arithmetic: 16.4 us -> 0.92 us
    all_gather x7 -> x0, waiting for transfers between devices: 430 us -> none  [the longest x4 171 us: prefix_by_axis(): lax.all_gather(part.astype(kind), axis)]
    pallas_call x0 -> x4, Pallas kernels: none -> 118 us  [the longest x1 53.5 us: gather_call(): pl.pallas_call(gather_kernel, out_shape=(jax.ShapeDtypeStruct((count, Z,...]
    dot_general x145 -> x0, matrix products: 89.5 us -> none  [the longest x136 78.2 us: matmul_high(): return jnp.matmul(left_side, right_side, precision=highest)]
    all_gather x8 -> x0, blocking collectives: 54.2 us -> none  [prefix_by_axis(): lax.all_gather(part.astype(kind), axis)]
    reshape x21 -> x4, local copies, waits for them, and re-layouts: 50.7 us -> 0.13 us  [the longest x1 0.08 us: on_device(): shift = lax.dynamic_slice_in_dim(beta_shift, first, 2, 1).reshape(4, 1)]
    gather x18 -> x0, local copies, waits for them, and re-layouts: 22.5 us -> none  [unit_lower_inverse(): jnp.diagonal(block_grid, axis1=-4, axis2=-2)]
    all_to_all x1 -> x0, blocking collectives: 18.4 us -> none  [sent_and_summed(): lax.all_to_all(tiles, axis, split_axis=0, concat_axis=0, tiled=True)]
    all_to_all x2 -> x0, waiting for transfers between devices: 10.4 us -> none  [sent_to_all(): return lax.all_to_all(copies, axis, split_axis=0, concat_axis=0, tiled=True)]
  transfers between devices with their start and end apart: 11 -> 0, of which waited for: 8 -> 0; matrix products, arithmetic and copies ran while one was open for 26% -> 0% of each run, Pallas kernels for 0% -> 0%
where the time goes in v1:
time: 135 us
  Pallas kernels  118 us (87%)
  local copies, waits for them, and re-layouts  15.6 us (12%)
    pallas_call x1, Pallas kernels, gather_call(): pl.pallas_call(gather_kernel, out_shape=(jax.ShapeDtypeStruct((count, Z,...  53.5 us
    pallas_call x1, Pallas kernels, carried_call(): pl.pallas_call(carried_kernel, out_shape=(jax.ShapeDtypeStruct((8, 64, HE...  31.6 us
    pallas_call x1, Pallas kernels, final_call(): pl.pallas_call(final_kernel, out_shape=jax.ShapeDtypeStruct((64, 2048), B...  16.6 us
    pallas_call x1, Pallas kernels, local_call(): pl.pallas_call(local_kernel, out_shape=(jax.ShapeDtypeStruct((2, 2, 2, PA...  16.5 us
    unnamed x27, local copies, waits for them, and re-layouts  9.04 us
    slice x1, local copies, waits for them, and re-layouts, on_device(): weights[:5]  3.82 us

profile of v1, /device:TPU:1, one launch (start us, length us, event | category | flops | bytes accessed | tf_op | source)
XLA Modules:
  0.0 134.8 jit_solution(12451456677762924327)
XLA Ops:
  0.0 0.0 copy-start
  0.0 0.9 fusion.1
  1.0 0.0 copy-done
  1.0 0.1 constant_dynamic-slice_fusion
  1.0 0.1 reshape.35.shift_ref
  1.1 0.7 constant_dynamic-update-slice_fusion.6
  1.8 0.7 constant_dynamic-update-slice_fusion.5
  2.5 0.7 constant_dynamic-update-slice_fusion.4
  3.2 0.7 constant_dynamic-update-slice_fusion.3
  3.9 0.7 constant_dynamic-update-slice_fusion.2
  4.6 0.7 constant_dynamic-update-slice_fusion.1
  5.3 0.7 constant_dynamic-update-slice_fusion.w_ref
  6.0 0.0 copy-start.3
  6.0 0.9 copy-done.3
  7.0 53.5 %gather.1 = (bf16[7,16,4,2,16,256]{5,4,3,2,1,0:T(8,128)(2,1)S(1)}, bf16[4,256,512]{2,1,0:T(8,128)(2,1)S(1)}) custom-call(bf16[7,16,256]{2,1,0:T(8,128)(2,1)S(1)} %constant_dynamic-update-slice_fusion.w_ref, bf16[256,512]{1,0:T(8,128)(2,1)S(1)} %copy-done.3), custom_call_target="tpu_custom_call" | custom-call | tf_op jit(solution)/shard_map/gather/pallas_call | solution.py:201
  60.4 0.0 copy-start.2
  60.5 0.0 copy-start.8
  60.5 0.0 copy-start.9
  60.5 0.0 copy-start.5
  60.5 3.8 %slice.12 = bf16[5,16,4,2,16,256]{5,4,3,2,1,0:T(8,128)(2,1)} slice(bf16[7,16,4,2,16,256]{5,4,3,2,1,0:T(8,128)(2,1)S(1)} %get-tuple-element.14), slice={[0:5], [0:16], [0:4], [0:2], [0:16], [0:256]} | slice | bytes 10485760 | tf_op jit(solution)/shard_map/slice | solution.py:685
  64.3 0.7 copy-done.2
  65.0 0.0 copy-start.4
  65.0 0.0 copy-start.6
  65.0 0.0 copy-done.8
  65.0 0.0 copy-done.9
  65.0 0.0 copy-done.5
  65.1 0.0 copy-start.1
  65.1 2.5 %copy-done.1 = bf16[5,16,4,2,16,256]{5,4,3,2,1,0:T(8,128)(2,1)S(1)} copy-done((bf16[5,16,4,2,16,256]{5,4,3,2,1,0:T(8,128)(2,1)S(1)}, bf16[5,16,4,2,16,256]{5,4,3,2,1,0:T(8,128)(2,1)}, u32[]{:S(2)}) %copy-start.1) | copy-done | bytes 5242904
  67.5 0.0 copy-start.7
  67.5 16.5 %local.1 = (bf16[2,2,2,208,128]{4,3,2,1,0:T(8,128)(2,1)S(1)}, bf16[2,2,256,128]{3,2,1,0:T(8,128)(2,1)S(1)}, f32[2,256,128]{2,1,0:T(8,128)S(1)}, bf16[256,256]{1,0:T(8,128)(2,1)S(1)}) custom-call(bf16[4,256,512]{2,1,0:T(8,128)(2,1)S(1)} %get-tuple-element.13.f_ref, f32[4,1,512]{2,1,0:T(1,128)S(1)} %bitcast.31, bf16[5,2048,256]{2,1,0:T(8,128)(2,1)S(1)} %bitcast.28, ...), custom_call_target="tpu_custom_call" | custom-call | tf_op jit(solution)/shard_map/local/pallas_call | solution.py:338
  84.0 0.0 copy-done.4
  84.0 0.0 copy-done.6
  84.0 31.6 %carried.1 = (bf16[8,64,128]{2,1,0:T(8,128)(2,1)S(1)}, bf16[256,256]{1,0:T(8,128)(2,1)S(1)}) custom-call(bf16[8,208,128]{2,1,0:T(8,128)(2,1)S(1)} %bitcast.30, bf16[256,256]{1,0:T(8,128)(2,1)S(1)} %get-tuple-element.16.gated_ref, bf16[31,256]{1,0:T(8,128)(2,1)S(1)} %copy-done.4, f32[1,256]{1,0:T(1,128)S(1)} %bitcast.32), custom_call_target="tpu_custom_call" | custom-call | tf_op jit(solution)/shard_map/carried/pallas_call | solution.py:561
  115.7 1.9 %slice.14 = bf16[2,16,4,2,16,256]{5,4,3,2,1,0:T(8,128)(2,1)S(1)} slice(bf16[7,16,4,2,16,256]{5,4,3,2,1,0:T(8,128)(2,1)} %copy-done.2), slice={[5:7], [0:16], [0:4], [0:2], [0:16], [0:256]} | slice | bytes 4194304 | tf_op jit(solution)/shard_map/slice | solution.py:694
  117.5 0.0 copy-done.7
  117.6 16.6 %final.1 = bf16[64,2048]{1,0:T(8,128)(2,1)S(1)} custom-call(bf16[8,64,128]{2,1,0:T(8,128)(2,1)S(1)} %get-tuple-element.17.entry_ref, bf16[2,2,256,128]{3,2,1,0:T(8,128)(2,1)S(1)} %get-tuple-element.18.reach_ref, f32[2,256,128]{2,1,0:T(8,128)S(1)} %get-tuple-element.19.offset_ref, bf16[256,256]{1,0:T(8,128)(2,1)S(1)} %get-tuple-element.20.conv_ref, ...), custom_call_target="tpu_custom_call" | custom-call | tf_op jit(solution)/shard_map/final/pallas_call | solution.py:627
  134.1 0.7 copy.26
  (3 shorter events, 0.0 us)
Async XLA Ops:
  0.0 1.0 copy-start
  6.0 0.9 copy-start.3
  60.4 4.6 %copy-start.2 = (bf16[7,16,4,2,16,256]{5,4,3,2,1,0:T(8,128)(2,1)}, bf16[7,16,4,2,16,256]{5,4,3,2,1,0:T(8,128)(2,1)S(1)}, u32[]{:S(2)}) copy-start(bf16[7,16,4,2,16,256]{5,4,3,2,1,0:T(8,128)(2,1)S(1)} %get-tuple-element.14) | copy-start | bytes 22020100
  60.5 4.6 %copy-start.8 = (f32[2,2,256]{2,1,0:T(2,128)S(1)}, f32[2,2,256]{2,1,0:T(2,128)}, u32[]{:S(2)}) copy-start(f32[2,2,256]{2,1,0:T(2,128)} %param.25) | copy-start | bytes 12292
  60.5 4.6 %copy-start.9 = (f32[2,2,256]{2,1,0:T(2,128)S(1)}, f32[2,2,256]{2,1,0:T(2,128)}, u32[]{:S(2)}) copy-start(f32[2,2,256]{2,1,0:T(2,128)} %param.26) | copy-start | bytes 12292
  60.5 4.6 %copy-start.5 = (f32[2048]{0:T(1024)S(1)}, f32[2048]{0:T(1024)}, u32[]{:S(2)}) copy-start(f32[2048]{0:T(1024)} %param.18) | copy-start | bytes 24580
  65.0 19.0 %copy-start.4 = (bf16[31,256]{1,0:T(8,128)(2,1)S(1)}, bf16[31,256]{1,0:T(8,128)(2,1)}, u32[]{:S(2)}) copy-start(bf16[31,256]{1,0:T(8,128)(2,1)} %taps_ref.1) | copy-start | bytes 47620
  65.0 19.0 %copy-start.6 = (f32[256]{0:T(256)S(1)}, f32[256]{0:T(256)}, u32[]{:S(2)}) copy-start(f32[256]{0:T(256)} %param.31) | copy-start | bytes 3076
  65.1 2.5 %copy-start.1 = (bf16[5,16,4,2,16,256]{5,4,3,2,1,0:T(8,128)(2,1)S(1)}, bf16[5,16,4,2,16,256]{5,4,3,2,1,0:T(8,128)(2,1)}, u32[]{:S(2)}) copy-start(bf16[5,16,4,2,16,256]{5,4,3,2,1,0:T(8,128)(2,1)} %slice.12) | copy-start | bytes 15728644
  67.5 50.0 %copy-start.7 = (f32[128]{0:T(128)S(1)}, f32[128]{0:T(128)}, u32[]{:S(2)}) copy-start(f32[128]{0:T(128)} %param.27) | copy-start | bytes 1540

commit v2 on v1

v2 whole, which is shorter than its diff:
```python
import jax
import jax.numpy as jnp
from jax import lax
from jax.experimental import pallas as pl
from jax.experimental.pallas import tpu as pltpu
from jax.sharding import Mesh
from jax.sharding import PartitionSpec as P

HEAD = 128
V_HEADS = 8
CONV_CH = 1024
KERNEL = 31
SP = ("sp_0", "sp_1", "sp_2")
SP_TP = ("sp_0", "sp_1", "sp_2", "tp")
Z, X, C, Y = (16, 4, 2, 4)
ROWS = 256
WIDE = 256
F32 = jnp.float32
BF16 = jnp.bfloat16
HIGHEST = lax.Precision.HIGHEST
MESH = pl.DeviceIdType.MESH
VMEM = pl.BlockSpec(memory_space=pltpu.VMEM)
PACKET = 208


def place():
    return tuple(lax.axis_index(a) for a in SP_TP)


def remote(src, dst, send, recv, to):
    return pltpu.make_async_remote_copy(
        src_ref=src, dst_ref=dst, send_sem=send, recv_sem=recv, device_id=to, device_id_type=MESH
    )


def greet(peers):
    barrier = pltpu.get_barrier_semaphore()
    for peer in peers:
        pl.semaphore_signal(barrier, inc=1, device_id=peer, device_id_type=MESH)
    pl.semaphore_wait(barrier, len(peers))


def bdot(a, b, dims):
    return lax.dot_general(
        a.astype(BF16), b.astype(BF16), (dims, ((), ())), preferred_element_type=F32
    )


def fdot(a, b, dims):
    return lax.dot_general(a, b, (dims, ((), ())), precision=HIGHEST, preferred_element_type=F32)


def triangle(lower, strict):
    i = lax.broadcasted_iota(jnp.int32, (ROWS, ROWS), 0)
    j = lax.broadcasted_iota(jnp.int32, (ROWS, ROWS), 1)
    if lower:
        return i > j if strict else i >= j
    return i < j if strict else i <= j


def silu(v):
    return v * jax.nn.sigmoid(v)


def mixing_terms(k, q, v, kk, qk, b_col, c_col, c_row, lower):
    mask = triangle(lower, False)
    gap = jnp.where(mask, jnp.exp(jnp.where(mask, c_col - c_row, 0.0)), 0.0)
    below = jnp.where(triangle(lower, True), b_col * kk * gap, 0.0)
    return (qk * gap).astype(BF16), below


def grow_inverse(below, inverse, size):
    i = lax.broadcasted_iota(jnp.int32, (ROWS, ROWS), 0)
    j = lax.broadcasted_iota(jnp.int32, (ROWS, ROWS), 1)
    twice = 2 * size
    pair = ((i & -twice) == (j & -twice)) & ((i & size) != (j & size))
    corner = jnp.where(pair, below, 0.0).astype(BF16)
    if size == 1:
        return (i == j).astype(BF16) - corner
    inner = bdot(corner, inverse, ((1,), (0,)))
    return inverse - bdot(inverse, inner, ((1,), (0,))).astype(BF16)


def corrected_inverse(below, inverse):
    i = lax.broadcasted_iota(jnp.int32, (ROWS, ROWS), 0)
    j = lax.broadcasted_iota(jnp.int32, (ROWS, ROWS), 1)
    high = below.astype(BF16)
    low = (below - high.astype(F32)).astype(BF16)
    product = bdot(high, inverse, ((1,), (0,))) + bdot(low, inverse, ((1,), (0,)))
    wide = inverse.astype(F32)
    residual = (i == j).astype(F32) - wide - product
    return (wide + bdot(inverse, residual, ((1,), (0,)))).astype(BF16)


def unpack(ref, at):
    body = ref[at].astype(F32)
    return (body[0:192], body[192:193] + body[200:201])


def joined(first, second):
    (body1, a1), (body2, a2) = (first, second)
    turned = bdot(body1, body2[0:128], ((1,), (0,)))
    top = a1 * body2[0:128] + a2 * body1[0:128] - turned[0:128]
    bottom = a2 * body1[128:192] - turned[128:192] + body2[128:192]
    return (jnp.concatenate([top, bottom], axis=0), a1 * a2)


def layer_kernel(
    x_hbm, qw, kw, vw, gvw, ggw, odw, ocw, bw_hbm, dw_hbm, gain_hbm, shift_hbm, pace_hbm, jolt_hbm,
    taps_hbm, norm_hbm, head_hbm, out_ref,
    x_ref, mine, bw, dw, gain_ref, shift_ref, pace_ref, jolt_ref, taps_ref, norm_ref, head_ref,
    g1, g2, f_ref, gate_rows, normed, packet_ref, reach_ref, offset_ref, gated_ref,
    parts, landed, passing, entry_ref, conv_ref,
    slab, before, leaving, near, far, parting, halo, stats, line, wide, filtered,
    zs, zr, xs, xr, ds, dr, ys, yr, us, ur, vs, vr,
    ss, sr, ns, nr, fs, fr, es, er, hs, hr, ts, tr, ps, pr, own,
):
    fetches = [(x_hbm, x_ref)]
    fetches += [(ref, mine.at[n]) for n, ref in enumerate((qw, kw, vw, gvw, ggw, odw, ocw))]
    fetches += [(bw_hbm, bw), (dw_hbm, dw), (gain_hbm, gain_ref), (shift_hbm, shift_ref)]
    fetches += [(pace_hbm, pace_ref), (jolt_hbm, jolt_ref), (taps_hbm, taps_ref)]
    fetches += [(norm_hbm, norm_ref), (head_hbm, head_ref)]
    z, x, c, y = place()
    xp, xm = (lax.rem(x + 1, X), lax.rem(x + X - 1, X))
    opp = lax.rem(x + 2, X)
    right, left = ((z, xp, c, y), (z, xm, c, y))
    other = (z, x, 1 - c, y)
    mates = [(z, x, c, lax.rem(y + d, Y)) for d in (2, 1, 3)]

    def on_z(d):
        return (lax.rem(z + d + Z, Z), x, c, y)

    fetched = [pltpu.make_async_copy(*pair, own.at[3 + n]) for n, pair in enumerate(fetches)]
    for copy in fetched:
        copy.start()
    near[...] = jnp.zeros_like(near)
    far[...] = jnp.zeros_like(far)
    greet([on_z(1), on_z(-1), on_z(2), on_z(-2), right, left, other] + mates)
    for copy in fetched:
        copy.wait()

    groups = (g1, g2)
    own_rows = (mine.at[0:3], mine.at[3:7])

    def behind(s):
        return lax.rem(z + Z - s, Z)

    def ahead(s):
        return lax.rem(z + s, Z)

    def z_copy(g, src, zi, s, way, to):
        return remote(src, groups[g].at[:, zi, x, c], zs.at[g, s, way], zr.at[g, s, way], to)

    def z_in(g, s, way):
        zi = behind(s) if way == 0 else ahead(s)
        ref = groups[g].at[:, zi, x, c]
        z_copy(g, ref, zi, s, way, right).wait_recv()

    def z_on(g, s, way, d):
        zi = behind(s) if way == 0 else ahead(s)
        src = own_rows[g] if s == 0 else groups[g].at[:, zi, x, c]
        z_copy(g, src, zi, s + d, way, on_z(d if way == 0 else -d)).start()

    def chunk(zi, xi):
        return g1.at[:, zi, xi, c]

    def x_copy(src, zi, xi, s, way, to):
        return remote(src, chunk(zi, xi), xs.at[s, way], xr.at[s, way], to)

    def d_copy(zi, ci, s, way):
        line = g1.at[:, zi, :, ci]
        return remote(line, line, ds.at[s, way], dr.at[s, way], other)

    def spread_p(s, src):
        x_copy(src, behind(s), x, s, 0, right).start()
        x_copy(src, behind(s), x, s, 1, left).start()

    def spread_q(s):
        src = chunk(ahead(s), x)
        x_copy(src, ahead(s), x, s, 2, left).start()
        x_copy(src, ahead(s), x, s, 3, right).start()

    def forward(s, both):
        p = chunk(behind(s), xm)
        x_copy(p, behind(s), xm, s, 0, right).wait_recv()
        x_copy(p, behind(s), xm, s, 4, right).start()
        if both:
            q = chunk(ahead(s), xp)
            x_copy(q, ahead(s), xp, s, 2, left).wait_recv()
            x_copy(q, ahead(s), xp, s, 5, left).start()

    def across(s, both):
        x_copy(chunk(behind(s), xp), behind(s), xp, s, 1, left).wait_recv()
        x_copy(chunk(behind(s), opp), behind(s), opp, s, 4, right).wait_recv()
        d_copy(behind(s), c, s, 0).start()
        if both:
            x_copy(chunk(ahead(s), xm), ahead(s), xm, s, 3, right).wait_recv()
            x_copy(chunk(ahead(s), opp), ahead(s), opp, s, 5, left).wait_recv()
            d_copy(ahead(s), c, s, 1).start()

    for way in (0, 1):
        z_on(0, 0, way, 2)
        z_on(0, 0, way, 1)
    spread_p(0, own_rows[0])
    feature_copies = []
    for i, mate in enumerate(mates):
        copy = remote(x_ref, f_ref.at[y], ys.at[i], yr.at[i], mate)
        copy.start()
        feature_copies.append(copy)
    for way in (0, 1):
        z_on(1, 0, way, 2)
        z_on(1, 0, way, 1)
    keeps = [
        pltpu.make_async_copy(own_rows[0], g1.at[:, z, x, c], own.at[0]),
        pltpu.make_async_copy(own_rows[1], g2.at[:, z, x, c], own.at[1]),
        pltpu.make_async_copy(x_ref, f_ref.at[y], own.at[2]),
    ]
    for copy in keeps:
        copy.start()
    for copy in keeps:
        copy.wait()

    def z_round(r):
        s = 2 * r
        z_in(0, s, 0)
        if s < 8:
            z_on(0, s, 0, 2)
            z_on(0, s, 0, 1)
            z_in(0, s, 1)
            if s < 6:
                z_on(0, s, 1, 2)
            z_on(0, s, 1, 1)
        z_in(0, s - 1, 0)
        z_in(0, s - 1, 1)
        spread_p(s, chunk(behind(s), x))
        if s < 8:
            spread_q(s)
        spread_p(s - 1, chunk(behind(s - 1), x))
        spread_q(s - 1)

    def z_round_later(r):
        s = 2 * r
        z_in(1, s, 0)
        if s < 8:
            z_on(1, s, 0, 2)
            z_on(1, s, 0, 1)
            z_in(1, s, 1)
            if s < 6:
                z_on(1, s, 1, 2)
            z_on(1, s, 1, 1)
        z_in(1, s - 1, 0)
        z_in(1, s - 1, 1)

    z_round(1)
    forward(0, False)
    z_round_later(1)
    z_round(2)
    forward(2, True)
    forward(1, True)
    across(0, False)
    z_round_later(2)
    z_round(3)
    forward(4, True)
    forward(3, True)
    across(2, True)
    across(1, True)
    z_round_later(3)
    z_round(4)
    forward(6, True)
    forward(5, True)
    across(4, True)
    across(3, True)
    forward(8, False)
    forward(7, True)
    z_round_later(4)

    def column(n, xi, ci):
        return g2.at[2 * n : 2 * n + 2, :, xi, ci]

    def half_column(n, xi, k):
        return g2.at[2 * n : 2 * n + 2, 8 * k : 8 * k + 8, xi, c]

    def u_copy(n, xi, way, to):
        return remote(column(n, xi, c), column(n, xi, c), us.at[n, way], ur.at[n, way], to)

    def u_half(n, xi, way, to):
        line = half_column(n, xi, way)
        return remote(line, line, us.at[n, 2 + way], ur.at[n, 2 + way], to)

    def v_copy(n, xi, ci, k):
        return remote(column(n, xi, ci), column(n, xi, ci), vs.at[n, k], vr.at[n, k], other)

    def later_open(n):
        u_copy(n, x, 0, right).start()
        u_copy(n, x, 1, left).start()
        v_copy(n, x, c, 0).start()

    def later_turn(n):
        u_copy(n, xm, 0, right).wait_recv()
        u_half(n, xm, 0, right).start()
        u_copy(n, xp, 1, left).wait_recv()
        u_half(n, xp, 1, left).start()
        v_copy(n, xm, c, 1).start()
        v_copy(n, xp, c, 2).start()

    def later_close(n):
        u_half(n, opp, 0, right).wait_recv()
        u_half(n, opp, 1, left).wait_recv()
        v_copy(n, opp, c, 3).start()

    def later_end(n):
        for k, xi in enumerate((x, xm, xp, opp)):
            v_copy(n, xi, 1 - c, k).wait_recv()

    later_open(0)
    for i, mate in enumerate(mates):
        src_y = lax.rem(y + Y - (2, 1, 3)[i], Y)
        remote(x_ref, f_ref.at[src_y], ys.at[i], yr.at[i], mate).wait_recv()

    total = jnp.zeros((ROWS, 1), F32)
    for p in range(Y):
        total = total + jnp.sum(f_ref[p].astype(F32), axis=1, keepdims=True)
    mean = total / 2048.0
    total = jnp.zeros((ROWS, 1), F32)
    for p in range(Y):
        total = total + jnp.sum(jnp.square(f_ref[p].astype(F32) - mean), axis=1, keepdims=True)
    scale = lax.rsqrt(total / 2048.0 + 1e-05)
    for p in range(Y):
        normed[:, p * 512 : (p + 1) * 512] = (
            (f_ref[p].astype(F32) - mean) * scale * gain_ref[p]
        ).astype(BF16)
    across(6, True)
    across(5, True)
    across(8, False)
    across(7, True)
    i = lax.broadcasted_iota(jnp.int32, (V_HEADS, V_HEADS), 0)
    j = lax.broadcasted_iota(jnp.int32, (V_HEADS, V_HEADS), 1)
    eye = (i == j).astype(F32)
    turned_shift = fdot(eye, shift_ref[...], ((1,), (1,)))
    for e in range(2):
        for n, ref in ((e, bw), (2 + e, dw)):
            every_head = bdot(ref[e], normed[...], ((1,), (1,)))
            if n < 2:
                every_head = jax.nn.sigmoid(every_head + turned_shift[:, e : e + 1])
            for k in range(V_HEADS):
                gate_rows[n, k] = every_head[k : k + 1]
    first = y * 2

    def two_heads(n):
        return jnp.concatenate([gate_rows[n, first], gate_rows[n, first + 1]], axis=0)

    beta = jnp.concatenate([two_heads(0), two_heads(1)], axis=0)
    pre = jnp.concatenate([two_heads(2), two_heads(3)], axis=0)
    soft = jnp.maximum(pre, 0.0) + jnp.log1p(jnp.exp(-jnp.abs(pre)))
    pace = jnp.concatenate([pace_ref[0], pace_ref[1]], axis=0)
    jolt = jnp.concatenate([jolt_ref[0], jolt_ref[1]], axis=0)
    log_decay = -pace * soft + jolt
    upto = triangle(False, False).astype(F32)
    since = triangle(True, False).astype(F32)
    padded = jnp.concatenate([log_decay, jnp.zeros((4, ROWS), F32)], axis=0)
    forth = fdot(padded, upto, ((1,), (0,)))
    back = fdot(padded, since, ((1,), (0,)))
    cumulative = jnp.concatenate([forth[0:2], back[2:4]], axis=0)
    lines = jnp.concatenate([beta, cumulative], axis=0)
    columns = jnp.transpose(lines)

    def d_arrived(s, way):
        d_copy(behind(s) if way == 0 else ahead(s), 1 - c, s, way).wait_recv()

    d_arrived(0, 0)

    @pl.loop(1, 8)
    def _(s):
        d_arrived(s, 0)
        d_arrived(s, 1)

    d_arrived(8, 0)

    def project(ref, n):
        weight = ref[n].reshape(2048, WIDE)
        return bdot(normed[...], weight, ((1,), (0,))).astype(BF16).astype(F32)

    query_all, key_all, value_all = (project(g1, 0), project(g1, 1), project(g1, 2))
    chains = []
    for h in range(2):
        lanes = slice(h * HEAD, (h + 1) * HEAD)
        q = silu(query_all[:, lanes])
        k = silu(key_all[:, lanes])
        k = k * lax.rsqrt(jnp.sum(jnp.square(k), axis=1, keepdims=True) + 1e-06)
        v = value_all[:, lanes]
        kk = bdot(k, k, ((1,), (1,)))
        qk = bdot(q, k, ((1,), (1,)))
        for e in range(2):
            n = e * 2 + h
            b_col = columns[:, n : n + 1]
            c_col = columns[:, 4 + n : 5 + n]
            c_row = cumulative[n : n + 1, :]
            scores, below = mixing_terms(k, q, v, kk, qk, b_col, c_col, c_row, e == 0)
            chains.append((h, e, q, k, v, b_col, c_col, c_row, scores, below))
    inverses = [None] * 4
    size = 1
    while size < ROWS:
        inverses = [grow_inverse(t[9], inv, size) for t, inv in zip(chains, inverses)]
        size = 2 * size
        if size == 16:
            later_turn(0)
            later_open(1)
    inverses = [corrected_inverse(t[9], inv) for t, inv in zip(chains, inverses)]
    within = [jnp.zeros((ROWS, HEAD), F32)] * 2
    for (h, e, q, k, v, b_col, c_col, c_row, scores, below), inverse in zip(chains, inverses):
        grown = jnp.exp(c_col)
        rhs = jnp.concatenate([v * b_col, k * (b_col * grown)], axis=1)
        both = bdot(inverse, rhs, ((1,), (0,))).astype(BF16)
        read = bdot(scores, both, ((1,), (0,)))
        within[h] = within[h] + read[:, :HEAD]
        reach_ref[e, h] = (q * grown - read[:, HEAD:]).astype(BF16)
        last = c_row[:, ROWS - 1 : ROWS] if e == 0 else c_row[:, 0:1]
        tail = k * jnp.exp(last - c_col)
        maps = bdot(both, tail, ((0,), (0,)))
        whole = jnp.broadcast_to(jnp.exp(last), (8, HEAD))
        high = whole.astype(BF16).astype(F32)
        scalars = jnp.concatenate([high, whole - high], axis=0).astype(BF16)
        for half in range(2):
            n = e * 4 + h * 2 + half
            packet_ref[n, 0:128] = maps[128:256].astype(BF16)
            packet_ref[n, 128:192] = maps[half * 64 : half * 64 + 64].astype(BF16)
            packet_ref[n, 192:208] = scalars
    for h in range(2):
        offset_ref[h] = within[h]

    step = 1 - 2 * c
    owner = c * X + x
    position = z * 8 + x * 2 + c
    spot = x * 2 + c

    def slab_peer(dx, dc):
        return (z, lax.rem(x + dx, X), c if dc == 0 else 1 - c, y)

    offsets = [(dx, dc) for dx in range(X) for dc in range(C) if (dx, dc) != (0, 0)]
    offsets = sorted(offsets, key=lambda o: -(2 if o[0] == 2 else min(o[0], 1)))

    def at_position(s):
        s = lax.rem(s + 128, 128)
        return (s // 8, lax.rem(s // 2, X), lax.rem(s, 2), y)

    following, preceding = (at_position(position + 1), at_position(position - 1))
    slab_copies = []
    for i, (dx, dc) in enumerate(offsets):
        to = slab_peer(dx, dc)
        copy = remote(
            packet_ref.at[to[2] * X + to[1]], slab.at[spot], ss.at[i], sr.at[i], to
        )
        copy.start()
        slab_copies.append(copy)
    slab[spot] = packet_ref[owner]
    later_close(0)
    later_turn(1)
    later_end(0)
    gated_ref[...] = (project(g2, 0) * jax.nn.sigmoid(project(g2, 1))).astype(BF16)
    halo_copies = [
        remote(gated_ref.at[ROWS - 16 : ROWS], halo.at[0], hs.at[0], hr.at[0], following),
        remote(gated_ref.at[0:16], halo.at[1], hs.at[1], hr.at[1], preceding),
    ]
    for copy in halo_copies:
        copy.start()

    for i, (dx, dc) in enumerate(offsets):
        source = slab_peer(X - dx, dc)
        remote(
            packet_ref.at[owner], slab.at[source[1] * 2 + source[2]], ss.at[i], sr.at[i], source
        ).wait_recv()

    def nth(t):
        return jnp.where(c == 0, t, 7 - t)

    running = unpack(slab, nth(0))
    for t in range(1, 8):
        before[t, 0:192] = running[0].astype(BF16)
        parting[t] = running[1]
        running = joined(running, unpack(slab, nth(t)))

    def pack(ref, value):
        body, a = value
        high = a.astype(BF16).astype(F32)
        ref[0:192] = body.astype(BF16)
        ref[192:208] = jnp.concatenate(
            [jnp.broadcast_to(high, (8, HEAD)), jnp.broadcast_to(a - high, (8, HEAD))], axis=0
        ).astype(BF16)

    def hop(d):
        return z + step * d

    def inside(d):
        return (hop(d) >= 0) & (hop(d) < Z)

    def z_peer(d):
        return (jnp.clip(hop(d), 0, Z - 1), x, c, y)

    def near_copy(i, d):
        return remote(leaving.at[0], near.at[i], ns.at[i], nr.at[i], z_peer(d))

    def far_copy(i, d):
        return remote(leaving.at[1], far.at[i], fs.at[i], fr.at[i], z_peer(d))

    pack(leaving.at[0], running)
    for i, d in ((2, 3), (1, 2), (0, 1)):

        @pl.when(inside(d))
        def _():
            near_copy(i, d).start()

    wide[16 : 16 + ROWS] = gated_ref[...].astype(F32)
    for copy in halo_copies:
        copy.wait_recv()
    wide[0:16] = halo[0].astype(F32) * (position > 0).astype(F32)
    wide[16 + ROWS : 32 + ROWS] = halo[1].astype(F32) * (position < 127).astype(F32)
    taps = taps_ref[...].astype(F32)

    @pl.loop(0, ROWS // 32)
    def _(r):
        window = wide[pl.ds(pl.multiple_of(r * 32, 32), 64)]
        total = jnp.zeros((32, WIDE), F32)
        for j in range(KERNEL):
            total = total + window[j + 1 : j + 33] * taps[j : j + 1]
        filtered[pl.ds(pl.multiple_of(r * 32, 32), 32)] = total

    ones = jnp.ones((8, WIDE), F32)
    whole = filtered[...]
    line[0:8] = fdot(ones, whole, ((1,), (1,)))
    line[8:16] = fdot(ones, whole * whole, ((1,), (1,)))
    stat_copies = []
    for i, mate in enumerate(mates):
        copy = remote(line, stats.at[i], ts.at[i], tr.at[i], mate)
        copy.start()
        stat_copies.append(copy)

    window = running
    for i, d in ((0, 1), (1, 2), (2, 3)):

        @pl.when(inside(-d))
        def _():
            near_copy(i, d).wait_recv()

        window = joined(unpack(near, i), window)
    pack(leaving.at[1], window)
    reaches = ((2, 9), (1, 5), (3, 13), (0, 1))
    for i, d in reaches:

        @pl.when(inside(d))
        def _():
            far_copy(i, d).start()

    for copy in stat_copies:
        copy.wait_recv()
    summed = line[...] + stats[0] + stats[1] + stats[2]
    spread = jnp.full((8, WIDE), 0.125, F32)
    mean = fdot(summed[0:8], spread, ((0,), (0,))) / CONV_CH
    second = fdot(summed[8:16], spread, ((0,), (0,))) / CONV_CH
    conv_ref[...] = silu(
        (filtered[...] - mean) * lax.rsqrt(second - mean * mean + 1e-05) * norm_ref[...]
    ).astype(BF16)

    later_close(1)

    @pl.when(inside(-1))
    def _():
        far_copy(0, 1).wait_recv()

    entering = unpack(far, 0)
    for i, d in ((1, 5), (2, 9), (3, 13)):

        @pl.when(inside(-d))
        def _():
            far_copy(i, d).wait_recv()

        entering = joined(unpack(far, i), entering)
    state = entering[0][128:192]
    line_up = [state]
    for t in range(1, 8):
        body = before[t].astype(F32)
        line_up.append(
            parting[t] * state - bdot(state, body[0:128], ((1,), (0,))) + body[128:192]
        )
    for t in range(8):
        slab[nth(t), 0:64] = line_up[t].astype(BF16)
    entry_ref[owner] = slab[spot, 0:64]
    entry_copies = []
    for i, (dx, dc) in enumerate(offsets):
        to = slab_peer(dx, dc)
        copy = remote(
            slab.at[to[1] * 2 + to[2], 0:64], entry_ref.at[owner], es.at[i], er.at[i], to
        )
        copy.start()
        entry_copies.append(copy)
    for i, (dx, dc) in enumerate(offsets):
        source = slab_peer(X - dx, dc)
        remote(
            slab.at[0, 0:64], entry_ref.at[source[2] * X + source[1]], es.at[i], er.at[i], source
        ).wait_recv()
    later_end(1)
    heads = []
    for h in range(2):
        o = offset_ref[h]
        for e in range(2):
            at = e * 4 + h * 2
            state = jnp.concatenate([entry_ref[at], entry_ref[at + 1]], axis=0)
            o = o + bdot(reach_ref[e, h], state, ((1,), (1,)))
        scale = lax.rsqrt(jnp.mean(jnp.square(o), axis=1, keepdims=True) + 1e-06)
        heads.append((o * scale * head_ref[...]).astype(BF16))
    delta = jnp.concatenate(heads, axis=1)
    conv = conv_ref[...]
    beside, facing = (y + 1 - 2 * lax.rem(y, 2), 3 - y)
    opposite = lax.rem(y + 2, Y)
    ways = ((beside, facing), (facing, beside))
    for n in range(2):
        a = g2[2].reshape(2048, WIDE)[n * 1024 : (n + 1) * 1024]
        b = g2[3].reshape(2048, WIDE)[n * 1024 : (n + 1) * 1024]
        total = bdot(delta, a, ((1,), (1,))) + bdot(conv, b, ((1,), (1,)))
        for p in range(Y):
            parts[n, p] = total[p * 64 : (p + 1) * 64].astype(BF16)

    def part_copy(n, k, block):
        to = (z, x, c, ways[n][0])
        return remote(parts.at[n, block], landed.at[n, k], ps.at[n, k], pr.at[n, k], to)

    def pass_copy(n):
        to = (z, x, c, ways[n][1])
        return remote(passing.at[n], landed.at[n, 2], ps.at[n, 2], pr.at[n, 2], to)

    for n in range(2):
        part_copy(n, 0, opposite).start()
    for n in range(2):
        part_copy(n, 1, ways[n][0]).start()
    for n in range(2):
        part_copy(n, 0, opposite).wait_recv()
        passing[n] = (parts[n, ways[n][1]].astype(F32) + landed[n, 0].astype(F32)).astype(BF16)
        pass_copy(n).start()
    for n in range(2):
        part_copy(n, 1, y).wait_recv()
        pass_copy(n).wait_recv()
        out_ref[:, n * 1024 : (n + 1) * 1024] = (
            parts[n, y].astype(F32) + landed[n, 1].astype(F32) + landed[n, 2].astype(F32)
        ).astype(BF16)
    for n in range(2):
        part_copy(n, 0, opposite).wait_send()
        part_copy(n, 1, y).wait_send()
        pass_copy(n).wait_send()
    for copy in slab_copies + halo_copies + stat_copies + entry_copies:
        copy.wait_send()
    for i, d in ((0, 1), (1, 2), (2, 3)):

        @pl.when(inside(d))
        def _():
            near_copy(i, d).wait_send()

    for i, d in reaches:

        @pl.when(inside(d))
        def _():
            far_copy(i, d).wait_send()

    def sent(s, both, zed):
        p, q = (chunk(behind(s), x), chunk(ahead(s), x))
        for g in (0, 1) if zed else ():
            for way in (0, 1) if both else (0,):
                ref = groups[g].at[:, behind(s), x, c]
                z_copy(g, ref, behind(s), s, way, right).wait_send()
        for way in (0, 1, 4) + ((2, 3, 5) if both else ()):
            x_copy(p, behind(s), x, s, way, right).wait_send()
        d_copy(behind(s), c, s, 0).wait_send()
        if both:
            d_copy(ahead(s), c, s, 1).wait_send()

    sent(0, False, False)

    @pl.loop(1, 8)
    def _(s):
        sent(s, True, True)

    sent(8, False, True)
    for copy in feature_copies:
        copy.wait_send()
    for n in range(2):
        u_copy(n, x, 0, right).wait_send()
        u_copy(n, x, 1, left).wait_send()
        u_half(n, xm, 0, right).wait_send()
        u_half(n, xp, 1, left).wait_send()
        for k in range(4):
            v_copy(n, x, c, k).wait_send()


def layer_call(arrays):
    dma = pltpu.SemaphoreType.DMA
    anywhere = pl.BlockSpec(memory_space=pl.ANY)
    vmem = pltpu.VMEM
    return pl.pallas_call(
        layer_kernel,
        out_shape=jax.ShapeDtypeStruct((64, 2048), BF16),
        in_specs=[anywhere] * len(arrays),
        out_specs=VMEM,
        scratch_shapes=[
            vmem((ROWS, 512), BF16), vmem((7, 16, WIDE), BF16),
            vmem((2, V_HEADS, 2048), BF16), vmem((2, V_HEADS, 2048), BF16),
            vmem((Y, 1, 512), F32), vmem((2, V_HEADS), F32), vmem((2, 2, ROWS), F32),
            vmem((2, 2, ROWS), F32), vmem((KERNEL, WIDE), BF16), vmem((1, WIDE), F32),
            vmem((1, HEAD), F32),
            vmem((3, Z, X, C, 16, WIDE), BF16), vmem((4, Z, X, C, 16, WIDE), BF16),
            vmem((Y, ROWS, 512), BF16), vmem((4, V_HEADS, 1, ROWS), F32),
            vmem((ROWS, 2048), BF16),
            vmem((8, PACKET, HEAD), BF16), vmem((2, 2, ROWS, HEAD), BF16),
            vmem((2, ROWS, HEAD), F32), vmem((ROWS, WIDE), BF16),
            vmem((2, Y, 64, 1024), BF16), vmem((2, 3, 64, 1024), BF16), vmem((2, 64, 1024), BF16),
            vmem((8, 64, HEAD), BF16), vmem((ROWS, WIDE), BF16),
            vmem((8, PACKET, HEAD), BF16), vmem((8, PACKET, HEAD), BF16),
            vmem((2, PACKET, HEAD), BF16), vmem((3, PACKET, HEAD), BF16),
            vmem((4, PACKET, HEAD), BF16), vmem((8, 1, HEAD), F32), vmem((2, 16, WIDE), BF16),
            vmem((3, 16, WIDE), F32), vmem((16, WIDE), F32), vmem((ROWS + 64, WIDE), F32),
            vmem((ROWS, WIDE), F32),
            dma((2, 9, 2)), dma((2, 9, 2)), dma((9, 6)), dma((9, 6)), dma((9, 2)), dma((9, 2)),
            dma((3,)), dma((3,)), dma((2, 4)), dma((2, 4)), dma((2, 4)), dma((2, 4)),
            dma((7,)), dma((7,)), dma((3,)), dma((3,)), dma((4,)), dma((4,)),
            dma((7,)), dma((7,)), dma((2,)), dma((2,)), dma((3,)), dma((3,)),
            dma((2, 3)), dma((2, 3)), dma((3 + len(arrays),)),
        ],
        compiler_params=pltpu.CompilerParams(
            collective_id=0, has_side_effects=True, vmem_limit_bytes=63 * 2**20
        ),
        name="layer",
    )(*arrays)


def on_device(
    inputs,
    in_gain,
    query_weight,
    key_weight,
    value_weight,
    beta_weight,
    decay_weight,
    beta_shift,
    decay_pace,
    decay_jolt,
    head_gain,
    glu_value_weight,
    glu_gate_weight,
    conv_kernel,
    conv_gain,
    out_delta_weight,
    out_conv_weight,
):
    return layer_call(
        [
            inputs,
            query_weight,
            key_weight,
            value_weight,
            glu_value_weight,
            glu_gate_weight,
            out_delta_weight.T,
            out_conv_weight.T,
            jnp.transpose(beta_weight, (0, 2, 1)),
            jnp.transpose(decay_weight, (0, 2, 1)),
            in_gain.reshape(Y, 1, 512),
            beta_shift,
            decay_pace,
            decay_jolt,
            conv_kernel,
            conv_gain.reshape(1, WIDE),
            head_gain.reshape(1, HEAD),
        ]
    )


def solution(mesh):
    finer = Mesh(mesh.devices.reshape(16, 4, 2, mesh.shape["tp"]), SP_TP)
    in_specs = (
        P(SP, "tp"),
        P(),
        P(SP, "tp"),
        P(SP, "tp"),
        P(SP, "tp"),
        P(),
        P(),
        P(),
        P(None, "tp", SP),
        P(None, "tp", SP),
        P(),
        P(SP, "tp"),
        P(SP, "tp"),
        P(None, "tp"),
        P("tp"),
        P("tp", SP),
        P("tp", SP),
    )
    return jax.shard_map(
        on_device, mesh=finer, in_specs=in_specs, out_specs=P(SP_TP, None), check_vma=False
    )
```

time: 135 us -> 97.1 us (0.72)
  Pallas kernels: 118 us -> 94.3 us
  local copies, waits for them, and re-layouts: 15.6 us -> 1.67 us
    pallas_call x4 -> x1, Pallas kernels: 118 us -> 94.3 us  [layer_call(): pl.pallas_call(layer_kernel, out_shape=jax.ShapeDtypeStruct((64, 2048), B...]
    unnamed x27 -> x1, local copies, waits for them, and re-layouts: 9.04 us -> 1.67 us
    slice x2 -> x0, local copies, waits for them, and re-layouts: 5.68 us -> none  [the longest x1 3.82 us: on_device(): weights[:5]]
where the time goes in v2:
time: 97.1 us; the launch traced here: 96 us
  Pallas kernels  94.3 us (97%)
  local copies, waits for them, and re-layouts  1.67 us (2%)
    pallas_call x1, Pallas kernels, layer_call(): pl.pallas_call(layer_kernel, out_shape=jax.ShapeDtypeStruct((64, 2048), B...  94.3 us

profile of v2, /device:TPU:1, one launch (start us, length us, event | category | flops | bytes accessed | tf_op | source)
XLA Modules:
  0.0 96.0 jit_solution(1566446033830512930)
XLA Ops:
  0.0 94.3 %layer.1 = bf16[64,2048]{1,0:T(8,128)(2,1)} custom-call(bf16[256,512]{1,0:T(8,128)(2,1)} %x_hbm.1, bf16[16,256]{1,0:T(8,128)(2,1)} %qw.1, bf16[16,256]{1,0:T(8,128)(2,1)} %kw.1, bf16[16,256]{1,0:T(8,128)(2,1)} %vw.1, bf16[16,256]{1,0:T(8,128)(2,1)} %gvw.1, bf16[16,256]{1,0:T(8,128)(2,1)} %ggw.1, bf16[16,256]{1,0:T(8,128)(2,1)} %bitcast.9, ...), custom_call_target="tpu_custom_call" | custom-call | tf_op jit(solution)/shard_map/layer/pallas_call | solution.py:696
  94.3 1.7 %copy.19 = bf16[64,2048]{1,0:T(8,128)(2,1)} copy(bf16[64,2048]{1,0:T(8,128)(2,1)} %layer.1) | data formatting | bytes 524288

commit v3 on v2

--- a/solution.py
+++ b/solution.py
@@ -135,7 +135,7 @@
         copy.start()
     near[...] = jnp.zeros_like(near)
     far[...] = jnp.zeros_like(far)
-    greet([on_z(1), on_z(-1), on_z(2), on_z(-2), right, left, other] + mates)
+    greet([on_z(1), on_z(-1), on_z(2), on_z(-2), right, left, other, (z, opp, c, y)] + mates)
     for copy in fetched:
         copy.wait()
 
@@ -202,11 +202,30 @@
         z_on(0, 0, way, 2)
         z_on(0, 0, way, 1)
     spread_p(0, own_rows[0])
-    feature_copies = []
-    for i, mate in enumerate(mates):
-        copy = remote(x_ref, f_ref.at[y], ys.at[i], yr.at[i], mate)
-        copy.start()
-        feature_copies.append(copy)
+    yp, ym = (lax.rem(y + 1, Y), lax.rem(y + Y - 1, Y))
+    facing_y = lax.rem(y + 2, Y)
+
+    def f_half(yi, half):
+        return f_ref.at[yi, half * 128 : half * 128 + 128]
+
+    def f_copy(way, half):
+        to = (z, x, c, yp if way == 0 else ym)
+        src = x_ref.at[half * 128 : half * 128 + 128]
+        return remote(src, f_half(y, half), ys.at[way, half], yr.at[way, half], to)
+
+    def f_arrived(way, half):
+        line = f_half(ym if way == 0 else yp, half)
+        remote(line, line, ys.at[way, half], yr.at[way, half], other).wait_recv()
+
+    def f_pass(way, yi):
+        line = f_half(yi, way)
+        to = (z, x, c, yp if way == 0 else ym)
+        return remote(line, line, ys.at[way, 2], yr.at[way, 2], to)
+
+    for way in (0, 1):
+        f_copy(way, way).start()
+    for way in (0, 1):
+        f_copy(way, 1 - way).start()
     for way in (0, 1):
         z_on(1, 0, way, 2)
         z_on(1, 0, way, 1)
@@ -252,27 +271,22 @@
         z_in(1, s - 1, 1)
 
     z_round(1)
+    z_round(2)
+    z_round_later(1)
     forward(0, False)
-    z_round_later(1)
-    z_round(2)
+    f_arrived(0, 0)
+    f_pass(0, ym).start()
+    f_arrived(1, 1)
+    f_pass(1, yp).start()
+    z_round(3)
+    z_round_later(2)
     forward(2, True)
     forward(1, True)
     across(0, False)
-    z_round_later(2)
-    z_round(3)
+    z_round(4)
     forward(4, True)
     forward(3, True)
-    across(2, True)
-    across(1, True)
     z_round_later(3)
-    z_round(4)
-    forward(6, True)
-    forward(5, True)
-    across(4, True)
-    across(3, True)
-    forward(8, False)
-    forward(7, True)
-    z_round_later(4)
 
     def column(n, xi, ci):
         return g2.at[2 * n : 2 * n + 2, :, xi, ci]
@@ -312,10 +326,10 @@
         for k, xi in enumerate((x, xm, xp, opp)):
             v_copy(n, xi, 1 - c, k).wait_recv()
 
-    later_open(0)
-    for i, mate in enumerate(mates):
-        src_y = lax.rem(y + Y - (2, 1, 3)[i], Y)
-        remote(x_ref, f_ref.at[src_y], ys.at[i], yr.at[i], mate).wait_recv()
+    f_arrived(0, 1)
+    f_arrived(1, 0)
+    for way in (0, 1):
+        f_pass(way, facing_y).wait_recv()
 
     total = jnp.zeros((ROWS, 1), F32)
     for p in range(Y):
@@ -329,21 +343,32 @@
         normed[:, p * 512 : (p + 1) * 512] = (
             (f_ref[p].astype(F32) - mean) * scale * gain_ref[p]
         ).astype(BF16)
+    forward(6, True)
+    forward(5, True)
+    across(2, True)
+    across(1, True)
+    forward(8, False)
+    forward(7, True)
+    across(4, True)
+    across(3, True)
+    z_round_later(4)
+    later_open(0)
     across(6, True)
     across(5, True)
-    across(8, False)
-    across(7, True)
     i = lax.broadcasted_iota(jnp.int32, (V_HEADS, V_HEADS), 0)
     j = lax.broadcasted_iota(jnp.int32, (V_HEADS, V_HEADS), 1)
     eye = (i == j).astype(F32)
     turned_shift = fdot(eye, shift_ref[...], ((1,), (1,)))
-    for e in range(2):
-        for n, ref in ((e, bw), (2 + e, dw)):
-            every_head = bdot(ref[e], normed[...], ((1,), (1,)))
-            if n < 2:
-                every_head = jax.nn.sigmoid(every_head + turned_shift[:, e : e + 1])
-            for k in range(V_HEADS):
-                gate_rows[n, k] = every_head[k : k + 1]
+    gate_weights = jnp.concatenate([bw[0], bw[1], dw[0], dw[1]], axis=0)
+    every_gate = bdot(gate_weights, normed[...], ((1,), (1,)))
+    for n in range(4):
+        every_head = every_gate[n * V_HEADS : (n + 1) * V_HEADS]
+        if n < 2:
+            every_head = jax.nn.sigmoid(every_head + turned_shift[:, n : n + 1])
+        for k in range(V_HEADS):
+            gate_rows[n, k] = every_head[k : k + 1]
+    across(8, False)
+    across(7, True)
     first = y * 2
 
     def two_heads(n):
@@ -404,7 +429,6 @@
         size = 2 * size
         if size == 16:
             later_turn(0)
-            later_open(1)
     inverses = [corrected_inverse(t[9], inv) for t, inv in zip(chains, inverses)]
     within = [jnp.zeros((ROWS, HEAD), F32)] * 2
     for (h, e, q, k, v, b_col, c_col, c_row, scores, below), inverse in zip(chains, inverses):
@@ -454,7 +478,6 @@
         slab_copies.append(copy)
     slab[spot] = packet_ref[owner]
     later_close(0)
-    later_turn(1)
     later_end(0)
     gated_ref[...] = (project(g2, 0) * jax.nn.sigmoid(project(g2, 1))).astype(BF16)
     halo_copies = [
@@ -473,6 +496,7 @@
     def nth(t):
         return jnp.where(c == 0, t, 7 - t)
 
+    later_open(1)
     running = unpack(slab, nth(0))
     for t in range(1, 8):
         before[t, 0:192] = running[0].astype(BF16)
@@ -550,6 +574,8 @@
         def _():
             far_copy(i, d).start()
 
+    later_turn(1)
+
     for copy in stat_copies:
         copy.wait_recv()
     summed = line[...] + stats[0] + stats[1] + stats[2]
@@ -560,7 +586,6 @@
         (filtered[...] - mean) * lax.rsqrt(second - mean * mean + 1e-05) * norm_ref[...]
     ).astype(BF16)
 
-    later_close(1)
 
     @pl.when(inside(-1))
     def _():
@@ -592,12 +617,14 @@
         )
         copy.start()
         entry_copies.append(copy)
+    later_close(1)
     for i, (dx, dc) in enumerate(offsets):
         source = slab_peer(X - dx, dc)
         remote(
             slab.at[0, 0:64], entry_ref.at[source[2] * X + source[1]], es.at[i], er.at[i], source
         ).wait_recv()
     later_end(1)
+
     heads = []
     for h in range(2):
         o = offset_ref[h]
@@ -612,22 +639,20 @@
     beside, facing = (y + 1 - 2 * lax.rem(y, 2), 3 - y)
     opposite = lax.rem(y + 2, Y)
     ways = ((beside, facing), (facing, beside))
+    def part_copy(n, k, block):
+        to = (z, x, c, ways[n][0])
+        return remote(parts.at[n, block], landed.at[n, k], ps.at[n, k], pr.at[n, k], to)
+
+    def pass_copy(n):
+        to = (z, x, c, ways[n][1])
+        return remote(passing.at[n], landed.at[n, 2], ps.at[n, 2], pr.at[n, 2], to)
+
     for n in range(2):
         a = g2[2].reshape(2048, WIDE)[n * 1024 : (n + 1) * 1024]
         b = g2[3].reshape(2048, WIDE)[n * 1024 : (n + 1) * 1024]
         total = bdot(delta, a, ((1,), (1,))) + bdot(conv, b, ((1,), (1,)))
         for p in range(Y):
             parts[n, p] = total[p * 64 : (p + 1) * 64].astype(BF16)
-
-    def part_copy(n, k, block):
-        to = (z, x, c, ways[n][0])
-        return remote(parts.at[n, block], landed.at[n, k], ps.at[n, k], pr.at[n, k], to)
-
-    def pass_copy(n):
-        to = (z, x, c, ways[n][1])
-        return remote(passing.at[n], landed.at[n, 2], ps.at[n, 2], pr.at[n, 2], to)
-
-    for n in range(2):
         part_copy(n, 0, opposite).start()
     for n in range(2):
         part_copy(n, 1, ways[n][0]).start()
@@ -678,8 +703,10 @@
         sent(s, True, True)
 
     sent(8, False, True)
-    for copy in feature_copies:
-        copy.wait_send()
+    for way in (0, 1):
+        f_copy(way, 0).wait_send()
+        f_copy(way, 1).wait_send()
+        f_pass(way, ym).wait_send()
     for n in range(2):
         u_copy(n, x, 0, right).wait_send()
         u_copy(n, x, 1, left).wait_send()
@@ -717,7 +744,7 @@
             vmem((3, 16, WIDE), F32), vmem((16, WIDE), F32), vmem((ROWS + 64, WIDE), F32),
             vmem((ROWS, WIDE), F32),
             dma((2, 9, 2)), dma((2, 9, 2)), dma((9, 6)), dma((9, 6)), dma((9, 2)), dma((9, 2)),
-            dma((3,)), dma((3,)), dma((2, 4)), dma((2, 4)), dma((2, 4)), dma((2, 4)),
+            dma((2, 3)), dma((2, 3)), dma((2, 4)), dma((2, 4)), dma((2, 4)), dma((2, 4)),
             dma((7,)), dma((7,)), dma((3,)), dma((3,)), dma((4,)), dma((4,)),
             dma((7,)), dma((7,)), dma((2,)), dma((2,)), dma((3,)), dma((3,)),
             dma((2, 3)), dma((2, 3)), dma((3 + len(arrays),)),

time: 97.1 us -> 91.4 us (0.941)
  Pallas kernels: 94.3 us -> 88.8 us
    pallas_call x1, Pallas kernels: 94.3 us -> 88.8 us  [layer_call(): pl.pallas_call(layer_kernel, out_shape=jax.ShapeDtypeStruct((64, 2048), B...]
where the time goes in v3:
time: 91.4 us; the launch traced here: 90.4 us
  Pallas kernels  88.8 us (97%)
  local copies, waits for them, and re-layouts  1.67 us (2%)
    pallas_call x1, Pallas kernels, layer_call(): pl.pallas_call(layer_kernel, out_shape=jax.ShapeDtypeStruct((64, 2048), B...  88.8 us

profile of v3, /device:TPU:1, one launch (start us, length us, event | category | flops | bytes accessed | tf_op | source)
XLA Modules:
  0.0 90.4 jit_solution(7018867929130328796)
XLA Ops:
  0.0 88.8 %layer.1 = bf16[64,2048]{1,0:T(8,128)(2,1)} custom-call(bf16[256,512]{1,0:T(8,128)(2,1)} %x_hbm.1, bf16[16,256]{1,0:T(8,128)(2,1)} %qw.1, bf16[16,256]{1,0:T(8,128)(2,1)} %kw.1, bf16[16,256]{1,0:T(8,128)(2,1)} %vw.1, bf16[16,256]{1,0:T(8,128)(2,1)} %gvw.1, bf16[16,256]{1,0:T(8,128)(2,1)} %ggw.1, bf16[16,256]{1,0:T(8,128)(2,1)} %bitcast.9, ...), custom_call_target="tpu_custom_call" | custom-call | tf_op jit(solution)/shard_map/layer/pallas_call | solution.py:723
  88.8 1.7 %copy.19 = bf16[64,2048]{1,0:T(8,128)(2,1)} copy(bf16[64,2048]{1,0:T(8,128)(2,1)} %layer.1) | data formatting | bytes 524288

commit v4 on v3

--- a/solution.py
+++ b/solution.py
@@ -130,7 +130,7 @@
     def on_z(d):
         return (lax.rem(z + d + Z, Z), x, c, y)
 
-    fetched = [pltpu.make_async_copy(*pair, own.at[3 + n]) for n, pair in enumerate(fetches)]
+    fetched = [pltpu.make_async_copy(*pair, own.at[4 + n]) for n, pair in enumerate(fetches)]
     for copy in fetched:
         copy.start()
     near[...] = jnp.zeros_like(near)
@@ -139,8 +139,8 @@
     for copy in fetched:
         copy.wait()
 
-    groups = (g1, g2)
-    own_rows = (mine.at[0:3], mine.at[3:7])
+    groups = (g1, g2.at[0:2], g2.at[2:4])
+    own_rows = (mine.at[0:3], mine.at[3:5], mine.at[5:7])
 
     def behind(s):
         return lax.rem(z + Z - s, Z)
@@ -231,7 +231,8 @@
         z_on(1, 0, way, 1)
     keeps = [
         pltpu.make_async_copy(own_rows[0], g1.at[:, z, x, c], own.at[0]),
-        pltpu.make_async_copy(own_rows[1], g2.at[:, z, x, c], own.at[1]),
+        pltpu.make_async_copy(own_rows[1], groups[1].at[:, z, x, c], own.at[1]),
+        pltpu.make_async_copy(own_rows[2], groups[2].at[:, z, x, c], own.at[3]),
         pltpu.make_async_copy(x_ref, f_ref.at[y], own.at[2]),
     ]
     for copy in keeps:
@@ -257,18 +258,18 @@
         spread_p(s - 1, chunk(behind(s - 1), x))
         spread_q(s - 1)
 
-    def z_round_later(r):
+    def z_round_later(r, g=1):
         s = 2 * r
-        z_in(1, s, 0)
+        z_in(g, s, 0)
         if s < 8:
-            z_on(1, s, 0, 2)
-            z_on(1, s, 0, 1)
-            z_in(1, s, 1)
+            z_on(g, s, 0, 2)
+            z_on(g, s, 0, 1)
+            z_in(g, s, 1)
             if s < 6:
-                z_on(1, s, 1, 2)
-            z_on(1, s, 1, 1)
-        z_in(1, s - 1, 0)
-        z_in(1, s - 1, 1)
+                z_on(g, s, 1, 2)
+            z_on(g, s, 1, 1)
+        z_in(g, s - 1, 0)
+        z_in(g, s - 1, 1)
 
     z_round(1)
     z_round(2)
@@ -287,6 +288,9 @@
     forward(4, True)
     forward(3, True)
     z_round_later(3)
+    for way in (0, 1):
+        z_on(2, 0, way, 2)
+        z_on(2, 0, way, 1)
 
     def column(n, xi, ci):
         return g2.at[2 * n : 2 * n + 2, :, xi, ci]
@@ -353,6 +357,7 @@
     across(3, True)
     z_round_later(4)
     later_open(0)
+    z_round_later(1, 2)
     across(6, True)
     across(5, True)
     i = lax.broadcasted_iota(jnp.int32, (V_HEADS, V_HEADS), 0)
@@ -405,6 +410,7 @@
         weight = ref[n].reshape(2048, WIDE)
         return bdot(normed[...], weight, ((1,), (0,))).astype(BF16).astype(F32)
 
+    z_round_later(2, 2)
     query_all, key_all, value_all = (project(g1, 0), project(g1, 1), project(g1, 2))
     chains = []
     for h in range(2):
@@ -429,6 +435,7 @@
         size = 2 * size
         if size == 16:
             later_turn(0)
+            z_round_later(3, 2)
     inverses = [corrected_inverse(t[9], inv) for t, inv in zip(chains, inverses)]
     within = [jnp.zeros((ROWS, HEAD), F32)] * 2
     for (h, e, q, k, v, b_col, c_col, c_row, scores, below), inverse in zip(chains, inverses):
@@ -477,6 +484,7 @@
         copy.start()
         slab_copies.append(copy)
     slab[spot] = packet_ref[owner]
+    z_round_later(4, 2)
     later_close(0)
     later_end(0)
     gated_ref[...] = (project(g2, 0) * jax.nn.sigmoid(project(g2, 1))).astype(BF16)
@@ -686,7 +694,7 @@
 
     def sent(s, both, zed):
         p, q = (chunk(behind(s), x), chunk(ahead(s), x))
-        for g in (0, 1) if zed else ():
+        for g in (0, 1, 2) if zed else ():
             for way in (0, 1) if both else (0,):
                 ref = groups[g].at[:, behind(s), x, c]
                 z_copy(g, ref, behind(s), s, way, right).wait_send()
@@ -743,11 +751,11 @@
             vmem((4, PACKET, HEAD), BF16), vmem((8, 1, HEAD), F32), vmem((2, 16, WIDE), BF16),
             vmem((3, 16, WIDE), F32), vmem((16, WIDE), F32), vmem((ROWS + 64, WIDE), F32),
             vmem((ROWS, WIDE), F32),
-            dma((2, 9, 2)), dma((2, 9, 2)), dma((9, 6)), dma((9, 6)), dma((9, 2)), dma((9, 2)),
+            dma((3, 9, 2)), dma((3, 9, 2)), dma((9, 6)), dma((9, 6)), dma((9, 2)), dma((9, 2)),
             dma((2, 3)), dma((2, 3)), dma((2, 4)), dma((2, 4)), dma((2, 4)), dma((2, 4)),
             dma((7,)), dma((7,)), dma((3,)), dma((3,)), dma((4,)), dma((4,)),
             dma((7,)), dma((7,)), dma((2,)), dma((2,)), dma((3,)), dma((3,)),
-            dma((2, 3)), dma((2, 3)), dma((3 + len(arrays),)),
+            dma((2, 3)), dma((2, 3)), dma((4 + len(arrays),)),
         ],
         compiler_params=pltpu.CompilerParams(
             collective_id=0, has_side_effects=True, vmem_limit_bytes=63 * 2**20

time: 91.4 us -> 89.4 us (0.978)
  the two profiles are of different devices: /device:TPU:1 before, /device:TPU:64 now
where the time goes in v4:
time: 89.4 us; the launch traced here: 89.2 us
  Pallas kernels  87.6 us (98%)
  local copies, waits for them, and re-layouts  1.67 us (2%)
    pallas_call x1, Pallas kernels, layer_call(): pl.pallas_call(layer_kernel, out_shape=jax.ShapeDtypeStruct((64, 2048), B...  87.6 us

profile of v4, /device:TPU:64, one launch (start us, length us, event | category | flops | bytes accessed | tf_op | source)
XLA Modules:
  0.0 89.2 jit_solution(10690302687765285476)
XLA Ops:
  0.0 87.6 %layer.1 = bf16[64,2048]{1,0:T(8,128)(2,1)} custom-call(bf16[256,512]{1,0:T(8,128)(2,1)} %x_hbm.1, bf16[16,256]{1,0:T(8,128)(2,1)} %qw.1, bf16[16,256]{1,0:T(8,128)(2,1)} %kw.1, bf16[16,256]{1,0:T(8,128)(2,1)} %vw.1, bf16[16,256]{1,0:T(8,128)(2,1)} %gvw.1, bf16[16,256]{1,0:T(8,128)(2,1)} %ggw.1, bf16[16,256]{1,0:T(8,128)(2,1)} %bitcast.9, ...), custom_call_target="tpu_custom_call" | custom-call | tf_op jit(solution)/shard_map/layer/pallas_call | solution.py:731
  87.6 1.7 %copy.19 = bf16[64,2048]{1,0:T(8,128)(2,1)} copy(bf16[64,2048]{1,0:T(8,128)(2,1)} %layer.1) | data formatting | bytes 524288
